TPU v7x, 32 devices: a whole 2x2x4 slice. The times are simulated.
32 devices in a mesh: ep: 8 (over z, core), tp: 4 (over y, x).
Axes of the slice: x: 2, y: 2, z: 4, core: 2. Of those that a mesh axis runs over, the one named last changes fastest.
Arguments:
- mixer_value_input: bfloat16 [2048, 4096], P('ep', 'tp'), may hold values from -6 to 6
- input_state_matrix: bfloat16 [2048, 2048], P('ep', 'tp'), may hold values from -6 to 6
- output_state_matrix: bfloat16 [2048, 2048], P('ep', 'tp'), may hold values from -6 to 6
- output_gate_input: bfloat16 [2048, 4096], P('ep', 'tp'), may hold values from -6 to 6
- step_input: float32 [2048, 64], P('ep', 'tp'), may hold values from -6 to -2
- extra_log_decay: float32 [2048, 64], P('ep', 'tp'), may hold values from -1 to 0
- head_log_decay: float32 [64], P('tp'), may hold values from -10 to 1
- head_skip_scale: float32 [64], P('tp'), may hold values from 0.5 to 2
- value_kernel: float32 [4, 4096], P(None, 'tp'), may hold values from -3 to 3
- input_matrix_kernel: float32 [4, 2048], P(None, 'tp'), may hold values from -3 to 3
- output_matrix_kernel: float32 [4, 2048], P(None, 'tp'), may hold values from -3 to 3
- mixer_norm_scale: float32 [4096], P('tp'), may hold values from 0.1 to 1.9
- mixer_output_weight: bfloat16 [4096, 2048], P(None, 'tp'), may hold values from -0.09375 to 0.09375
- second_token_rows: bfloat16 [2048, 2048], P('ep'), may hold values from -6 to 6
- expert_norm_scale: float32 [2048], replicated, may hold values from 0.1 to 1.9
- routed_expert_index: int32 [2048, 4], P('ep'), may hold values from 0 to 15, all different within a row; in each aligned block of 256 rows (0 to 255, 256 to 511, ...) at most 96 rows name the same one
- routed_expert_weight: float32 [2048, 4], P('ep'), may hold values from 0.1 to 1
- routed_gate_weight: bfloat16 [16, 2048, 1024], P('ep', None, 'tp'), may hold values from -0.125 to 0.125
- routed_up_weight: bfloat16 [16, 2048, 1024], P('ep', None, 'tp'), may hold values from -0.125 to 0.125
- routed_down_weight: bfloat16 [16, 1024, 2048], P('ep', None, 'tp'), may hold values from -0.1875 to 0.1875
- shared_gate_weight: bfloat16 [2048, 1024], P(None, 'tp'), may hold values from -0.125 to 0.125
- shared_up_weight: bfloat16 [2048, 1024], P(None, 'tp'), may hold values from -0.125 to 0.125
- shared_down_weight: bfloat16 [1024, 2048], P(None, 'tp'), may hold values from -0.1875 to 0.1875
Outputs:
- mixer_output: bfloat16 [2048, 2048], P('ep', 'tp')
- routed_out: bfloat16 [2048, 2048], P('ep', 'tp')
Inputs may be any that keep to these rules, and one draw needn't show every extreme that they name: `routed_expert_index`: in each aligned block of 256 rows (the rows of one index of ep) no expert is named more than 96 times, a bound that some block reaches.
All inputs are finite; a program needn't handle non-finite values.
Results may differ from a plain program's by a relative error of at most 0.012.
Values may be sent and summed in bfloat16 or wider, within the bound.
A program may use at most 64 MiB of HBM per device.

v0:
```python
import jax
import jax.numpy as jnp
from jax import lax
from jax.sharding import PartitionSpec as P

HEAD_DIM = 64
STATE = 128
CONV_TAPS = 4
BLOCK = 128
TOP_K = 4


epsilon = 1e-05
precise = lax.Precision.HIGHEST


def passed_along(x, axis, by):
    size = lax.axis_size(axis)
    pairs = [(i, i + by) for i in range(size) if 0 <= i + by < size]
    return lax.ppermute(x, axis, pairs)


def carried_in(x, axis, join, neutral):
    place = lax.axis_index(axis)
    gathered = jax.tree.map(
        lambda a, kind: lax.all_gather(a.astype(kind), axis), x, (jnp.bfloat16, jnp.bfloat16)
    )
    state = jax.tree.map(lambda a, e: jnp.zeros_like(a) + jnp.asarray(e, a.dtype), x, neutral)

    def one(turn, state):
        return join(
            state,
            jax.tree.map(
                lambda a, own: lax.dynamic_index_in_dim(a, turn, 0, False).astype(own.dtype),
                gathered,
                x,
            ),
        )

    return lax.fori_loop(0, place, one, state)


def conv_silu(tail_rows, source, weights):
    length = source.shape[0]
    padded = jnp.concatenate([tail_rows, source], axis=0)
    total_sum = jnp.zeros(source.shape, jnp.float32)
    for tap_index in range(CONV_TAPS):
        total_sum = (
            total_sum
            + padded[tap_index : tap_index + length].astype(jnp.float32) * weights[tap_index]
        )
    return jax.nn.silu(total_sum).astype(jnp.bfloat16)


def join_states(earlier, later_part):
    return (earlier[0] * later_part[0], later_part[0][:, None, None] * earlier[1] + later_part[1])


def carry_blocks(carried, inputs):
    block_decay, block_state = inputs
    return (carried * block_decay[:, None, None] + block_state, carried)


def route_slots(route_block, experts, capacity):
    flat_ids = route_block.reshape(-1)
    onehot = (flat_ids[:, None] == jnp.arange(experts, dtype=jnp.int32)[None, :]).astype(jnp.int32)
    earlier = jnp.cumsum(onehot, axis=0) - onehot
    position_in = jnp.sum(earlier * onehot, axis=1)
    slot_index = flat_ids * capacity + position_in
    owner_row = jnp.arange(flat_ids.shape[0], dtype=jnp.int32) // route_block.shape[1]
    slot_owner = (
        jnp.full((experts * capacity,), route_block.shape[0], jnp.int32)
        .at[slot_index]
        .set(owner_row)
    )
    return (slot_owner, slot_index)


def on_device(
    mixer_value_input,
    input_state_matrix,
    output_state_matrix,
    output_gate_input,
    step_input,
    extra_log_decay,
    head_log_decay,
    head_skip_scale,
    value_kernel,
    input_matrix_kernel,
    output_matrix_kernel,
    mixer_norm_scale,
    mixer_output_weight,
    second_token_rows,
    expert_norm_scale,
    routed_expert_index,
    routed_expert_weight,
    routed_gate_weight,
    routed_up_weight,
    routed_down_weight,
    shared_gate_weight,
    shared_up_weight,
    shared_down_weight,
):
    length = mixer_value_input.shape[0]
    heads_local = step_input.shape[1]
    width_x = mixer_value_input.shape[1]
    width_b = input_state_matrix.shape[1]
    groups_local = width_b // STATE
    head_ratio = heads_local // groups_local
    nblocks = length // BLOCK
    lead_row = length - CONV_TAPS + 1
    edge_rows = jnp.concatenate(
        [
            mixer_value_input[lead_row:],
            input_state_matrix[lead_row:],
            output_state_matrix[lead_row:],
        ],
        axis=1,
    )
    tail_rows = passed_along(edge_rows, "ep", 1)
    values = conv_silu(tail_rows[:, :width_x], mixer_value_input, value_kernel)
    in_mat = conv_silu(
        tail_rows[:, width_x : width_x + width_b], input_state_matrix, input_matrix_kernel
    )
    out_mat = conv_silu(
        tail_rows[:, width_x + width_b :], output_state_matrix, output_matrix_kernel
    )
    step_length = jax.nn.softplus(step_input)
    decay_logarithm = -jnp.exp(head_log_decay)[None, :] * step_length + extra_log_decay
    running = jnp.cumsum(decay_logarithm.reshape(nblocks, BLOCK, heads_local), axis=1)
    value_wide = values.astype(jnp.float32).reshape(nblocks, BLOCK, heads_local, HEAD_DIM)
    scaled = value_wide * step_length.reshape(nblocks, BLOCK, heads_local)[..., None]
    in_blocks = in_mat.reshape(nblocks, BLOCK, groups_local, STATE)
    out_blocks = out_mat.reshape(nblocks, BLOCK, groups_local, STATE)
    scores = jnp.einsum(
        "bign,bjgn->bgij", out_blocks, in_blocks, preferred_element_type=jnp.float32
    )
    scores = jnp.repeat(scores, head_ratio, axis=1)
    spread = jnp.transpose(running[:, :, None, :] - running[:, None, :, :], (0, 3, 1, 2))
    lower_mask = jnp.tril(jnp.ones((BLOCK, BLOCK), bool))[None, None]
    decay_mat = jnp.where(lower_mask, jnp.exp(jnp.where(lower_mask, spread, 0.0)), 0.0)
    inside = jnp.einsum("bhij,bjhp->bihp", scores * decay_mat, scaled, precision=precise)
    out_head = jnp.repeat(out_blocks.astype(jnp.float32), head_ratio, axis=2)
    in_head = jnp.repeat(in_blocks.astype(jnp.float32), head_ratio, axis=2)
    block_logs = running[:, -1]
    to_end = jnp.exp(block_logs[:, None, :] - running)
    block_state = jnp.einsum("bjhn,bjh,bjhp->bhpn", in_head, to_end, scaled, precision=precise)
    start_state = jnp.zeros((heads_local, HEAD_DIM, STATE), jnp.float32)
    local_total, local_prev = lax.scan(
        carry_blocks, start_state, (jnp.exp(block_logs), block_state)
    )
    before_logs = jnp.cumsum(block_logs, axis=0) - block_logs
    incoming = carried_in(
        (jnp.exp(jnp.sum(block_logs, axis=0)), local_total),
        "ep",
        join_states,
        (jnp.ones((heads_local,), jnp.float32), start_state),
    )
    entering = local_prev + jnp.exp(before_logs)[:, :, None, None] * incoming[1][None]
    carried_term = (
        jnp.einsum("bihn,bhpn->bihp", out_head, entering, precision=precise)
        * jnp.exp(running)[..., None]
    )
    mixed_heads = (inside + carried_term).reshape(length, heads_local, HEAD_DIM)
    mixed_heads = mixed_heads + head_skip_scale[None, :, None] * value_wide.reshape(
        length, heads_local, HEAD_DIM
    )
    gated_heads = mixed_heads * jax.nn.silu(output_gate_input.astype(jnp.float32)).reshape(
        length, heads_local, HEAD_DIM
    )
    grouped = gated_heads.reshape(length, groups_local, head_ratio * HEAD_DIM)
    grouped = grouped * lax.rsqrt(jnp.mean(grouped * grouped, axis=-1, keepdims=True) + epsilon)
    mixer_normed = (grouped.reshape(length, width_x) * mixer_norm_scale).astype(jnp.bfloat16)
    rows_local = second_token_rows.shape[0]
    model_width = second_token_rows.shape[1]
    local_experts = routed_gate_weight.shape[0]
    ep_count = lax.axis_size("ep")
    experts = local_experts * ep_count
    capacity = max(2, 3 * rows_local * TOP_K // (2 * experts))
    col_width = model_width // lax.axis_size("tp")
    rows_wide = second_token_rows.astype(jnp.float32)
    normed = (
        rows_wide
        * lax.rsqrt(jnp.mean(rows_wide * rows_wide, axis=-1, keepdims=True) + epsilon)
        * expert_norm_scale
    ).astype(jnp.bfloat16)
    slot_owner, slot_index = route_slots(routed_expert_index, experts, capacity)
    padded = jnp.concatenate([normed, jnp.zeros((1, model_width), jnp.bfloat16)], axis=0)
    outgoing = jnp.take(padded, slot_owner, axis=0).reshape(experts, capacity, model_width)
    my_columns = lax.dynamic_slice_in_dim(outgoing, lax.axis_index("tp") * col_width, col_width, 2)
    arrived = lax.all_to_all(my_columns, "ep", split_axis=0, concat_axis=1, tiled=True)
    column_piece = lax.all_gather(arrived, "tp", axis=2, tiled=True)
    gate_pre = jnp.einsum(
        "esd,edf->esf", column_piece, routed_gate_weight, preferred_element_type=jnp.float32
    )
    up_pre = jnp.einsum(
        "esd,edf->esf", column_piece, routed_up_weight, preferred_element_type=jnp.float32
    )
    hidden = (jax.nn.silu(gate_pre) * up_pre).astype(jnp.bfloat16)
    shared_hidden = (
        jax.nn.silu(jnp.dot(normed, shared_gate_weight, preferred_element_type=jnp.float32))
        * jnp.dot(normed, shared_up_weight, preferred_element_type=jnp.float32)
    ).astype(jnp.bfloat16)
    whole_mix, whole_hidden, whole_shared = (
        lax.all_gather(mixer_normed, "tp", axis=1, tiled=True),
        lax.all_gather(hidden, "tp", axis=2, tiled=True),
        lax.all_gather(shared_hidden, "tp", axis=1, tiled=True),
    )
    mixer_output = jnp.dot(
        whole_mix, mixer_output_weight, preferred_element_type=jnp.float32
    ).astype(jnp.bfloat16)
    expert_result = jnp.einsum(
        "esf,efd->esd", whole_hidden, routed_down_weight, preferred_element_type=jnp.float32
    ).astype(jnp.bfloat16)
    returned = lax.all_to_all(expert_result, "ep", split_axis=1, concat_axis=0, tiled=True)
    picked = jnp.take(returned.reshape(experts * capacity, col_width), slot_index, axis=0)
    picked = picked.reshape(rows_local, TOP_K, col_width).astype(jnp.float32)
    routed_sum = jnp.sum(picked * routed_expert_weight[:, :, None], axis=1)
    shared_result = jnp.dot(whole_shared, shared_down_weight, preferred_element_type=jnp.float32)
    routed_out = (routed_sum + shared_result).astype(jnp.bfloat16)
    return (mixer_output, routed_out)


def solution(mesh):
    return jax.shard_map(
        on_device,
        mesh=mesh,
        in_specs=(
            P("ep", "tp"),
            P("ep", "tp"),
            P("ep", "tp"),
            P("ep", "tp"),
            P("ep", "tp"),
            P("ep", "tp"),
            P("tp"),
            P("tp"),
            P(None, "tp"),
            P(None, "tp"),
            P(None, "tp"),
            P("tp"),
            P(None, "tp"),
            P("ep", None),
            P(),
            P("ep", None),
            P("ep", None),
            P("ep", None, "tp"),
            P("ep", None, "tp"),
            P("ep", None, "tp"),
            P(None, "tp"),
            P(None, "tp"),
            P(None, "tp"),
        ),
        out_specs=(P("ep", "tp"), P("ep", "tp")),
        check_vma=False,
    )
```

profile of v0, /device:TPU:0, one launch (start us, length us, event | category | flops | bytes accessed | tf_op | source)
XLA Modules:
  0.0 292.6 jit_solution(14076036180507357092)
XLA Ops:
  9.2 4.5 %reduce-window.6 = s32[16,8,128]{2,1,0:T(8,128)S(1)} reduce-window(s32[16,8,128]{2,1,0:T(8,128)S(1)} %fusion.50, s32[]{:T(128)} %constant.114.clone.1), window={size=1x1x128 pad=0_0x0_0x127_0}, to_apply=%region_8.9 | reduce-window | flops 2080768 | bytes 131076 | tf_op jit(solution)/shard_map/reduce-window
  15.6 4.3 %scatter_custom_fusion = s32[1536]{0:T(1024)S(1)} fusion(s32[1024]{0:T(1024)S(1)} %bitcast.142, s32[1024]{0:T(1024)S(1)} %add_select_fusion, s32[]{:T(128)} %constant.122.clone.1), kind=kCustom, calls=%fused_computation.105 | custom fusion | bytes 6148 | tf_op jit(solution)/shard_map/scatter | solution.py:74
  21.7 7.0 %gather_fusion = bf16[1536,2048]{1,0:T(8,128)(2,1)} fusion(bf16[257,2048]{1,0:T(8,128)(2,1)S(1)} %concatenate.19, s32[2048]{0:T(1024)S(1)} %pad_clamp_fusion), kind=kCustom, calls=%fused_computation | custom fusion | bytes 12589056 | tf_op jit(solution)/shard_map/jit(_take)/gather | solution.py:189
  30.6 43.9 %all_to_all.33 = bf16[16,96,512]{2,1,0:T(8,128)(2,1)S(1)} all-to-all(bf16[16,96,512]{2,1,0:T(8,128)(2,1)S(1)} %dynamic-slice_select_fusion), channel_id=1, replica_groups=mesh['ep'=8,'tp'=4] {'ep'}, dimensions={0} | all-to-all | bytes 3145728 | tf_op jit(solution)/shard_map/all_to_all | solution.py:191
  95.4 2.9 broadcast_multiply_fusion
  98.5 3.1 %fusion.26 = f32[2,16,64,128]{3,2,1,0:T(8,128)} fusion(f32[2,128,16,128]{3,1,2,0:T(8,128)S(1)} %bitcast.125, f32[2,128,16,64]{1,0,3,2:T(2,128)S(1)} %get-tuple-element.115), kind=kOutput, calls=%fused_computation.43 | convolution fusion | flops 402653184 | bytes 4194304 | tf_op jit(solution)/shard_map/bjhn,bjh,bjhp->bhpn/dot_general | solution.py:147
  101.6 4.1 %while.26 = (s32[]{:T(128)}, f32[16,64,128]{2,1,0:T(8,128)S(1)}, f32[2,16,64,128]{3,2,1,0:T(8,128)}, f32[2,16]{1,0:T(2,128)S(1)}, f32[2,16,64,128]{3,2,1,0:T(8,128)}, /*index=5*/s32[]{:T(128)}, s32[]{:T(128)}) while((s32[]{:T(128)}, f32[16,64,128]{2,1,0:T(8,128)S(1)}, f32[2,16,64,128]{3,2,1,0:T(8,128)}, f32[2,16]{1,0:T(2,128)S(1)}, ...), condition=%wide.region_2.3_spmd.clone, body=%wide.region_1.2_spmd.clone.sunk | while | flops 524291 | bytes 2622240 | solution.py:149
  106.7 38.1 %all-gather.9.cloned.1.call-done = bf16[2,768,2048]{2,1,0:T(8,128)(2,1)} async-done(((bf16[2,768,512]{2,1,0:T(8,128)(2,1)}), bf16[2,768,2048]{2,1,0:T(8,128)(2,1)}) %all-gather.9.cloned.1.call-update) | async-done | bytes 6291472 | tf_op jit(solution)/shard_map/all_gather | solution.py:192
  144.8 5.3 %fusion.62 = f32[2,768,256]{2,1,0:T(8,128)S(1)} fusion(bf16[2,768,2048]{2,1,0:T(8,128)(2,1)} %all-gather.9.cloned.1.call-done, bf16[2,2048,256]{2,1,0:T(8,128)(2,1)} %param.44), kind=kOutput, calls=%fused_computation.123 | convolution fusion | flops 1610612736 | bytes 9961472 | tf_op jit(solution)/shard_map/esd,edf->esf/dot_general | solution.py:193
  150.7 2.9 multiply_convert_fusion
  157.3 17.1 %all-reduce.1 = bf16[128]{0:T(256)(128)(2,1)S(1)} all-reduce(bf16[128]{0:T(256)(128)(2,1)S(1)} %dynamic-update-slice), channel_id=2, replica_groups=mesh['ep'=8,'tp'=4] {'ep'}, use_global_device_ids=true, to_apply=%add.1 | all-reduce | flops 128 | bytes 512
  181.6 4.2 %fusion.16 = f32[2,128,16,64]{1,3,2,0:T(8,128)S(1)} fusion(f32[2,128,16,128]{3,1,2,0:T(8,128)S(1)} %bitcast.126, f32[2,16,64,128]{3,2,1,0:T(8,128)S(1)} %copy-done.9, f32[2,128,16]{1,2,0:T(8,128)S(1)} %copy-done.14, f32[16,64,128]{2,1,0:T(8,128)S(1)} %get-tuple-element.76, f32[2,16]{1,0:T(2,128)S(1)} %copy-done.33), kind=kOutput, calls=%fused_computation.27 | convolution fusion | flops 403439616 | bytes 4735104 | tf_op jit(solution)/shard_map/bihn,bhpn->bihp/dot_general | solution.py:161
  187.1 4.2 %fusion.13 = f32[2,128,16,64]{1,3,2,0:T(8,128)S(1)} fusion(f32[2,128,16,64]{1,3,2,0:T(8,128)S(1)} %fusion.16, f32[2,16,128,128]{3,2,1,0:T(8,128)S(1)} %bitcast.124, f32[2,128,16,64]{1,0,3,2:T(2,128)S(1)} %copy-done.6, f32[2,16,128]{2,1,0:T(8,128)S(1)} %copy.106, pred[128,128]{1,0:T(8,128)(4,1)S(1)} %copy-done.13), kind=kOutput, calls=%fused_computation.25 | convolution fusion | flops 405012480 | bytes 5275648 | tf_op jit(solution)/shard_map/bhij,bjhp->bihp/dot_general | solution.py:142
  193.1 3.1 %reshape.204 = f32[256,4,256]{0,2,1:T(8,128)} reshape(f32[2,128,16,64]{1,0,3,2:T(2,128)} %copy.114) | data formatting | bytes 2097152 | tf_op jit(solution)/shard_map/reshape | solution.py:164
  199.6 21.9 %all-gather.11.cloned.1.call-done = bf16[2,768,1024]{2,1,0:T(8,128)(2,1)} async-done(((bf16[2,768,256]{2,1,0:T(8,128)(2,1)}), bf16[2,768,1024]{2,1,0:T(8,128)(2,1)}) %all-gather.11.cloned.1.call-update) | async-done | bytes 3145744 | tf_op jit(solution)/shard_map/all_gather | solution.py:206
  221.5 3.7 %convolution_convert_fusion = bf16[2,768,512]{2,1,0:T(8,128)(2,1)S(1)} fusion(bf16[2,768,1024]{2,1,0:T(8,128)(2,1)} %all-gather.11.cloned.1.call-done, bf16[2,1024,512]{2,1,0:T(8,128)(2,1)S(1)} %copy-done), kind=kOutput, calls=%fused_computation.21 | convolution fusion | flops 1611399168 | bytes 6815744 | tf_op jit(solution)/shard_map/esf,efd->esd/dot_general | solution.py:212
  227.9 5.0 %all-to-all-start.1 = ((bf16[2,768,512]{2,0,1:T(2,128)(2,1)}), bf16[2,768,512]{2,0,1:T(2,128)(2,1)}, u32[]{:S(2)}, u32[]{:S(2)}) async-start(bf16[2,768,512]{2,0,1:T(2,128)(2,1)} %copy.125), calls=%async_computation.1 | async-start | bytes 3145728 | tf_op jit(solution)/shard_map/all_to_all | solution.py:215
  235.7 20.6 %all_gather.28 = bf16[256,1024]{1,0:T(8,128)(2,1)} all-gather(bf16[256,256]{1,0:T(8,128)(2,1)S(1)} %fusion.18), channel_id=1, replica_groups=mesh['ep'=8,'tp'=4] {'tp'}, dimensions={1}, use_global_device_ids=true | all-gather | bytes 655360 | tf_op jit(solution)/shard_map/all_gather | solution.py:207
  256.3 6.2 %all-gather.7.cloned.1.call-done = bf16[256,4096]{0,1:T(8,128)(2,1)} async-done(((bf16[256,1024]{0,1:T(8,128)(2,1)}), bf16[256,4096]{0,1:T(8,128)(2,1)}) %all-gather.7.cloned.1.call-update) | async-done | bytes 2097168 | tf_op jit(solution)/shard_map/all_gather | solution.py:205
  262.6 4.8 %convolution_convert_fusion.1 = bf16[256,512]{1,0:T(8,128)(2,1)} fusion(bf16[256,4096]{0,1:T(8,128)(2,1)} %all-gather.7.cloned.1.call-done, bf16[4096,512]{1,0:T(8,128)(2,1)} %param.39), kind=kOutput, calls=%fused_computation.32 | convolution fusion | flops 1073872896 | bytes 6553600 | tf_op jit(solution)/shard_map/dot_general | solution.py:209
  267.3 3.5 %all-to-all-done.1 = bf16[2,768,512]{2,0,1:T(2,128)(2,1)} async-done(((bf16[2,768,512]{2,0,1:T(2,128)(2,1)}), bf16[2,768,512]{2,0,1:T(2,128)(2,1)}, u32[]{:S(2)}, u32[]{:S(2)}) %all-to-all-start.1) | async-done | bytes 1572896 | tf_op jit(solution)/shard_map/all_to_all | solution.py:215
  270.8 2.9 copy.126
  273.7 5.6 %gather_fusion.1 = bf16[1024,512]{1,0:T(8,128)(2,1)S(1)} fusion(bf16[1536,512]{1,0:T(8,128)(2,1)} %bitcast.121, s32[1024]{0:T(1024)S(1)} %broadcast_clamp_fusion), kind=kCustom, calls=%fused_computation.1 | custom fusion | bytes 2101248 | tf_op jit(solution)/shard_map/jit(_take)/gather | solution.py:216
  280.4 3.4 %multiply_reduce_fusion = f32[256,512]{1,0:T(8,128)S(1)} fusion(f32[256,4]{1,0:T(8,128)S(1)} %copy.127, bf16[256,4,512]{2,1,0:T(4,128)(2,1)} %gather.15, pred[256,4]{1,0:T(8,128)(4,1)S(1)} %copy.122), kind=kLoop, calls=%fused_computation.14 | loop fusion | flops 1966080 | bytes 1577984 | tf_op jit(solution)/shard_map/reduce_sum | solution.py:218
  (193 shorter events, 59.1 us)
Async XLA Ops:
  7.2 214.3 %copy-start = (bf16[2,1024,512]{2,1,0:T(8,128)(2,1)S(1)}, bf16[2,1024,512]{2,1,0:T(8,128)(2,1)}, u32[]{:S(2)}) copy-start(bf16[2,1024,512]{2,1,0:T(8,128)(2,1)} %param.46) | copy-start | bytes 6291460
  7.2 12.8 %copy-start.7 = (bf16[256,2048]{1,0:T(8,128)(2,1)S(1)}, bf16[256,2048]{1,0:T(8,128)(2,1)}, u32[]{:S(2)}) copy-start(bf16[256,2048]{1,0:T(8,128)(2,1)} %param.40) | copy-start | bytes 3145732
  7.2 13.2 %copy-start.25 = (f32[2048]{0:T(1024)S(1)}, f32[2048]{0:T(1024)}, u32[]{:S(2)}) copy-start(f32[2048]{0:T(1024)} %param.41) | copy-start | bytes 24580
  7.2 137.6 %all-gather.9.cloned.1.call-start = ((), (), s32[]{:S(2)}) async-start(), calls=%async_computation.3 | async-start | bytes 7864320 | tf_op jit(solution)/shard_map/all_gather | solution.py:192
  74.5 6.0 %copy-start.40 = (f32[16]{0:T(128)S(1)}, f32[16]{0:T(128)}, u32[]{:S(2)}) copy-start(f32[16]{0:T(128)} %param.33) | copy-start | bytes 196
  74.5 6.0 %copy-start.23 = (f32[256,16]{0,1:T(8,128)S(1)}, f32[256,16]{0,1:T(8,128)}, u32[]{:S(2)}) copy-start(f32[256,16]{0,1:T(8,128)} %param.31) | copy-start | bytes 49156
  74.5 6.0 %copy-start.24 = (f32[256,16]{0,1:T(8,128)S(1)}, f32[256,16]{0,1:T(8,128)}, u32[]{:S(2)}) copy-start(f32[256,16]{0,1:T(8,128)} %param.32) | copy-start | bytes 49156
  75.8 6.3 %copy-start.30 = (f32[4,512]{1,0:T(4,128)S(1)}, f32[4,512]{1,0:T(4,128)}, u32[]{:S(2)}) copy-start(f32[4,512]{1,0:T(4,128)} %param.36) | copy-start | bytes 24580
  75.8 6.9 %copy-start.22 = (f32[4,1024]{1,0:T(4,128)S(1)}, f32[4,1024]{1,0:T(4,128)}, u32[]{:S(2)}) copy-start(f32[4,1024]{1,0:T(4,128)} %param.35) | copy-start | bytes 49156
  75.8 104.3 %all-gather.13.cloned.1.call-start = ((), (), s32[]{:S(2)}) async-start(), calls=%async_computation.5 | async-start | bytes 2359296 | tf_op jit(solution)/shard_map/all_gather | solution.py:26
  78.4 7.2 %collective-permute-start = (bf16[3,2048]{0,1:T(8,128)(2,1)}, bf16[3,2048]{0,1:T(8,128)(2,1)}, u32[]{:S(2)}, u32[]{:S(2)}) collective-permute-start(bf16[3,2048]{0,1:T(8,128)(2,1)} %copy.98), channel_id=1, source_target_pairs={{0,4},{4,8},{8,12},{12,16},{16,20},{20,24},{24,28},{1,5},{5,9},{9,... | collective-permute-start | bytes 36872 | tf_op jit(solution)/shard_map/ppermute | solution.py:20
  106.5 115.0 %all-gather.11.cloned.1.call-start = ((), (), s32[]{:S(2)}) async-start(), calls=%async_computation.4 | async-start | bytes 3932160 | tf_op jit(solution)/shard_map/all_gather | solution.py:206
  144.8 5.4 %copy-start.37 = (bf16[2,768,2048]{2,1,0:T(8,128)(2,1)S(1)}, bf16[2,768,2048]{2,1,0:T(8,128)(2,1)}, u32[]{:S(2)}) copy-start(bf16[2,768,2048]{2,1,0:T(8,128)(2,1)} %all-gather.9.cloned.1.call-done) | copy-start | bytes 18874372
  144.8 5.8 %copy-start.38 = (bf16[2,2048,256]{2,1,0:T(8,128)(2,1)S(1)}, bf16[2,2048,256]{2,1,0:T(8,128)(2,1)}, u32[]{:S(2)}) copy-start(bf16[2,2048,256]{2,1,0:T(8,128)(2,1)} %param.45) | copy-start | bytes 6291460
  150.7 6.4 %copy-start.36 = (f32[16]{0:T(128)S(1)}, f32[16]{0:T(128)}, u32[]{:S(2)}) copy-start(f32[16]{0:T(128)} %get-tuple-element.119) | copy-start | bytes 196
  150.7 25.2 %copy-start.11 = (bf16[256,1024]{1,0:T(8,128)(2,1)S(1)}, bf16[256,1024]{1,0:T(8,128)(2,1)}, u32[]{:S(2)}) copy-start(bf16[256,1024]{1,0:T(8,128)(2,1)} %param.30) | copy-start | bytes 1572868
  153.6 25.0 %copy-start.12 = (bf16[256,512]{1,0:T(8,128)(2,1)S(1)}, bf16[256,512]{1,0:T(8,128)(2,1)}, u32[]{:S(2)}) copy-start(bf16[256,512]{1,0:T(8,128)(2,1)} %param.29) | copy-start | bytes 786436
  153.6 109.0 %all-gather.7.cloned.1.call-start = ((), (), s32[]{:S(2)}) async-start(), calls=%async_computation.2 | async-start | bytes 2621440 | tf_op jit(solution)/shard_map/all_gather | solution.py:205
  193.1 5.1 %copy-start.31 = (f32[1024]{0:T(1024)S(1)}, f32[1024]{0:T(1024)}, u32[]{:S(2)}) copy-start(f32[1024]{0:T(1024)} %param.38) | copy-start | bytes 12292
  227.9 5.2 %copy-start.17 = (s32[256,4]{0,1:T(4,128)S(1)}, s32[256,4]{0,1:T(4,128)}, u32[]{:S(2)}) copy-start(s32[256,4]{0,1:T(4,128)} %param.42) | copy-start | bytes 12292
  227.9 5.4 %copy-start.32 = (f32[256,4]{0,1:T(4,128)S(1)}, f32[256,4]{0,1:T(4,128)}, u32[]{:S(2)}) copy-start(f32[256,4]{0,1:T(4,128)} %param.43) | copy-start | bytes 12292
  227.9 5.6 %copy-start.3 = (bf16[256,2048]{1,0:T(8,128)(2,1)S(1)}, bf16[256,2048]{1,0:T(8,128)(2,1)}, u32[]{:S(2)}) copy-start(bf16[256,2048]{1,0:T(8,128)(2,1)} %copy-done.2) | copy-start | bytes 3145732
  227.9 42.9 %all-to-all-start.1 = ((bf16[2,768,512]{2,0,1:T(2,128)(2,1)}), bf16[2,768,512]{2,0,1:T(2,128)(2,1)}, u32[]{:S(2)}, u32[]{:S(2)}) async-start(bf16[2,768,512]{2,0,1:T(2,128)(2,1)} %copy.125), calls=%async_computation.1 | async-start | bytes 3145728 | tf_op jit(solution)/shard_map/all_to_all | solution.py:215
  235.3 21.0 %copy-start.21 = (s32[1024,1]{0,1:T(1,128)S(1)}, s32[1024,1]{0,1:T(1,128)}, u32[]{:S(2)}) copy-start(s32[1024,1]{0,1:T(1,128)} %copy-done.20) | copy-start | bytes 12292
  (23 other events, 60.7 us)
Sparse Core Ops, SparseCore 0:
  76.0 68.8 all-gather.8
  147.0 29.4 all-gather.12
  178.3 43.1 all-gather.10
  223.2 39.3 all-gather.6
where the time goes:
time: 294 us; the launch traced here: 293 us
  blocking collectives  81.7 us (28%)
  waiting for transfers between devices  69.8 us (24%)
  local copies, waits for them, and re-layouts  55.5 us (19%)
  matrix products  32.9 us (11%)
  other arithmetic  30 us (10%)
  between operations  15.1 us (5%)
  starting transfers between devices  7.51 us (3%)
    all_to_all x1, blocking collectives, on_device(): lax.all_to_all(my_columns, 'ep', split_axis=0, concat_axis=1, tiled=True)  43.9 us
    all_gather x1, waiting for transfers between devices, on_device(): column_piece = lax.all_gather(arrived, 'tp', axis=2, tiled=True)  38.1 us
    all_gather x1, waiting for transfers between devices, on_device(): lax.all_gather(hidden, 'tp', axis=2, tiled=True)  21.9 us
    all_gather x1, blocking collectives, on_device(): lax.all_gather(shared_hidden, 'tp', axis=1, tiled=True)  20.6 us
    unnamed x1, blocking collectives  17.1 us
    unnamed x89, local copies, waits for them, and re-layouts  7.6 us
    gather x1, local copies, waits for them, and re-layouts, on_device(): jnp.take(padded, slot_owner, axis=0).reshape(experts, capacity, model_width)  7.02 us
    gather x2, local copies, waits for them, and re-layouts, on_device(): jnp.take(returned.reshape(experts * capacity, col_width), slot_index, axi...  6.73 us
  transfers between devices with their start and end apart: 6, of which 4 were waited for; matrix products, arithmetic and copies ran while one was open for 26% of the time, Pallas kernels for 0%

commit v1 on v0

--- a/solution.py
+++ b/solution.py
@@ -20,24 +20,18 @@
     return lax.ppermute(x, axis, pairs)
 
 
-def carried_in(x, axis, join, neutral):
+def carried_in(total_log, state, axis):
+    size = lax.axis_size(axis)
     place = lax.axis_index(axis)
-    gathered = jax.tree.map(
-        lambda a, kind: lax.all_gather(a.astype(kind), axis), x, (jnp.bfloat16, jnp.bfloat16)
-    )
-    state = jax.tree.map(lambda a, e: jnp.zeros_like(a) + jnp.asarray(e, a.dtype), x, neutral)
-
-    def one(turn, state):
-        return join(
-            state,
-            jax.tree.map(
-                lambda a, own: lax.dynamic_index_in_dim(a, turn, 0, False).astype(own.dtype),
-                gathered,
-                x,
-            ),
-        )
-
-    return lax.fori_loop(0, place, one, state)
+    log = passed_along(total_log, axis, 1)
+    hold = passed_along(state.astype(jnp.bfloat16), axis, 1).astype(jnp.float32)
+    by = 1
+    while by < size - 1:
+        before = passed_along(hold.astype(jnp.bfloat16), axis, by).astype(jnp.float32)
+        hold = hold + jnp.exp(log)[:, None, None] * before
+        log = log + passed_along(log, axis, by)
+        by *= 2
+    return hold
 
 
 def conv_silu(tail_rows, source, weights):
@@ -52,28 +46,20 @@
     return jax.nn.silu(total_sum).astype(jnp.bfloat16)
 
 
-def join_states(earlier, later_part):
-    return (earlier[0] * later_part[0], later_part[0][:, None, None] * earlier[1] + later_part[1])
-
-
 def carry_blocks(carried, inputs):
     block_decay, block_state = inputs
     return (carried * block_decay[:, None, None] + block_state, carried)
 
 
-def route_slots(route_block, experts, capacity):
-    flat_ids = route_block.reshape(-1)
-    onehot = (flat_ids[:, None] == jnp.arange(experts, dtype=jnp.int32)[None, :]).astype(jnp.int32)
-    earlier = jnp.cumsum(onehot, axis=0) - onehot
-    position_in = jnp.sum(earlier * onehot, axis=1)
-    slot_index = flat_ids * capacity + position_in
-    owner_row = jnp.arange(flat_ids.shape[0], dtype=jnp.int32) // route_block.shape[1]
-    slot_owner = (
-        jnp.full((experts * capacity,), route_block.shape[0], jnp.int32)
-        .at[slot_index]
-        .set(owner_row)
-    )
-    return (slot_owner, slot_index)
+def earlier_counts(mask, rows):
+    at = jnp.arange(rows)
+    tri = (at[:, None] < at[None, :]).astype(jnp.bfloat16)
+    return lax.dot_general(
+        mask.astype(jnp.bfloat16),
+        tri,
+        (((mask.ndim - 1,), (0,)), ((), ())),
+        preferred_element_type=jnp.float32,
+    )
 
 
 def on_device(
@@ -118,12 +104,41 @@
         axis=1,
     )
     tail_rows = passed_along(edge_rows, "ep", 1)
-    values = conv_silu(tail_rows[:, :width_x], mixer_value_input, value_kernel)
+    rows_local = second_token_rows.shape[0]
+    model_width = second_token_rows.shape[1]
+    local_experts = routed_gate_weight.shape[0]
+    ep_count = lax.axis_size("ep")
+    experts = local_experts * ep_count
+    capacity = max(2, 3 * rows_local * TOP_K // (2 * experts))
+    col_width = model_width // lax.axis_size("tp")
+    rows_wide = second_token_rows.astype(jnp.float32)
+    normed = (
+        rows_wide
+        * lax.rsqrt(jnp.mean(rows_wide * rows_wide, axis=-1, keepdims=True) + epsilon)
+        * expert_norm_scale
+    ).astype(jnp.bfloat16)
+    ids = routed_expert_index.T.astype(jnp.float32)
+    id_rows = -(-ids.size // col_width)
+    id_block = jnp.pad(
+        ids.astype(jnp.bfloat16).reshape(-1), (0, id_rows * col_width - ids.size)
+    ).reshape(id_rows, col_width)
+    id_block = jnp.pad(id_block, ((0, -id_rows % 8), (0, 0)))
+    my_columns = lax.dynamic_slice_in_dim(normed, lax.axis_index("tp") * col_width, col_width, 1)
+    outgoing, value_rows, in_rows, out_rows = lax.optimization_barrier(
+        (
+            jnp.concatenate([my_columns, id_block], axis=0),
+            mixer_value_input,
+            input_state_matrix,
+            output_state_matrix,
+        )
+    )
+    everyone = lax.all_gather(outgoing, "ep", axis=0)
+    values = conv_silu(tail_rows[:, :width_x], value_rows, value_kernel)
     in_mat = conv_silu(
-        tail_rows[:, width_x : width_x + width_b], input_state_matrix, input_matrix_kernel
+        tail_rows[:, width_x : width_x + width_b], in_rows, input_matrix_kernel
     )
     out_mat = conv_silu(
-        tail_rows[:, width_x + width_b :], output_state_matrix, output_matrix_kernel
+        tail_rows[:, width_x + width_b :], out_rows, output_matrix_kernel
     )
     step_length = jax.nn.softplus(step_input)
     decay_logarithm = -jnp.exp(head_log_decay)[None, :] * step_length + extra_log_decay
@@ -150,13 +165,29 @@
         carry_blocks, start_state, (jnp.exp(block_logs), block_state)
     )
     before_logs = jnp.cumsum(block_logs, axis=0) - block_logs
-    incoming = carried_in(
-        (jnp.exp(jnp.sum(block_logs, axis=0)), local_total),
-        "ep",
-        join_states,
-        (jnp.ones((heads_local,), jnp.float32), start_state),
-    )
-    entering = local_prev + jnp.exp(before_logs)[:, :, None, None] * incoming[1][None]
+    everyone, local_total = lax.optimization_barrier((everyone, local_total))
+    incoming = carried_in(jnp.sum(block_logs, axis=0), local_total, "ep")
+    their_rows = everyone[:, :rows_local]
+    their_ids = everyone[:, rows_local : rows_local + id_rows].reshape(ep_count, -1)
+    their_ids = their_ids[:, : ids.size].reshape(ep_count, TOP_K, rows_local).astype(jnp.float32)
+    mine = (lax.axis_index("ep") * local_experts + jnp.arange(local_experts)).astype(jnp.float32)
+    named = jnp.any(their_ids[:, None] == mine[None, :, None, None], axis=2)
+    seat = jnp.where(named, earlier_counts(named, rows_local), -1.0)
+    seats = jnp.arange(capacity, dtype=jnp.float32)
+    pick = (seat[:, :, None, :] == seats[None, None, :, None]).astype(jnp.bfloat16)
+    arrived = jnp.stack(
+        [
+            jnp.einsum(
+                "bsr,brd->bsd", pick[:, j], their_rows, preferred_element_type=jnp.float32
+            )
+            .astype(jnp.bfloat16)
+            .reshape(ep_count * capacity, col_width)
+            for j in range(local_experts)
+        ]
+    )
+    column_piece = lax.all_gather(arrived, "tp", axis=2, tiled=True)
+    column_piece, incoming = lax.optimization_barrier((column_piece, incoming))
+    entering = local_prev + jnp.exp(before_logs)[:, :, None, None] * incoming[None]
     carried_term = (
         jnp.einsum("bihn,bhpn->bihp", out_head, entering, precision=precise)
         * jnp.exp(running)[..., None]
@@ -171,25 +202,6 @@
     grouped = gated_heads.reshape(length, groups_local, head_ratio * HEAD_DIM)
     grouped = grouped * lax.rsqrt(jnp.mean(grouped * grouped, axis=-1, keepdims=True) + epsilon)
     mixer_normed = (grouped.reshape(length, width_x) * mixer_norm_scale).astype(jnp.bfloat16)
-    rows_local = second_token_rows.shape[0]
-    model_width = second_token_rows.shape[1]
-    local_experts = routed_gate_weight.shape[0]
-    ep_count = lax.axis_size("ep")
-    experts = local_experts * ep_count
-    capacity = max(2, 3 * rows_local * TOP_K // (2 * experts))
-    col_width = model_width // lax.axis_size("tp")
-    rows_wide = second_token_rows.astype(jnp.float32)
-    normed = (
-        rows_wide
-        * lax.rsqrt(jnp.mean(rows_wide * rows_wide, axis=-1, keepdims=True) + epsilon)
-        * expert_norm_scale
-    ).astype(jnp.bfloat16)
-    slot_owner, slot_index = route_slots(routed_expert_index, experts, capacity)
-    padded = jnp.concatenate([normed, jnp.zeros((1, model_width), jnp.bfloat16)], axis=0)
-    outgoing = jnp.take(padded, slot_owner, axis=0).reshape(experts, capacity, model_width)
-    my_columns = lax.dynamic_slice_in_dim(outgoing, lax.axis_index("tp") * col_width, col_width, 2)
-    arrived = lax.all_to_all(my_columns, "ep", split_axis=0, concat_axis=1, tiled=True)
-    column_piece = lax.all_gather(arrived, "tp", axis=2, tiled=True)
     gate_pre = jnp.einsum(
         "esd,edf->esf", column_piece, routed_gate_weight, preferred_element_type=jnp.float32
     )
@@ -201,21 +213,42 @@
         jax.nn.silu(jnp.dot(normed, shared_gate_weight, preferred_element_type=jnp.float32))
         * jnp.dot(normed, shared_up_weight, preferred_element_type=jnp.float32)
     ).astype(jnp.bfloat16)
-    whole_mix, whole_hidden, whole_shared = (
-        lax.all_gather(mixer_normed, "tp", axis=1, tiled=True),
-        lax.all_gather(hidden, "tp", axis=2, tiled=True),
-        lax.all_gather(shared_hidden, "tp", axis=1, tiled=True),
-    )
+    slots = ep_count * capacity
+    hidden_rows = jnp.concatenate(
+        [hidden.reshape(local_experts * slots, hidden.shape[2]), shared_hidden], axis=0
+    )
+    whole_rows = lax.all_gather(hidden_rows, "tp", axis=1, tiled=True)
+    whole_hidden = whole_rows[: local_experts * slots].reshape(local_experts, slots, -1)
+    whole_shared = whole_rows[local_experts * slots :]
+    whole_mix = lax.all_gather(mixer_normed, "tp", axis=1, tiled=True)
     mixer_output = jnp.dot(
         whole_mix, mixer_output_weight, preferred_element_type=jnp.float32
     ).astype(jnp.bfloat16)
     expert_result = jnp.einsum(
         "esf,efd->esd", whole_hidden, routed_down_weight, preferred_element_type=jnp.float32
     ).astype(jnp.bfloat16)
-    returned = lax.all_to_all(expert_result, "ep", split_axis=1, concat_axis=0, tiled=True)
-    picked = jnp.take(returned.reshape(experts * capacity, col_width), slot_index, axis=0)
-    picked = picked.reshape(rows_local, TOP_K, col_width).astype(jnp.float32)
-    routed_sum = jnp.sum(picked * routed_expert_weight[:, :, None], axis=1)
+    going = jnp.concatenate(
+        [expert_result[j].reshape(ep_count, capacity, col_width) for j in range(local_experts)],
+        axis=1,
+    )
+    returned = lax.all_to_all(going, "ep", split_axis=0, concat_axis=0, tiled=True)
+    returned = returned.reshape(experts * capacity, col_width)
+    kinds = jnp.arange(experts, dtype=jnp.float32)
+    chosen = ids[:, None, :] == kinds[None, :, None]
+    count = earlier_counts(jnp.any(chosen, axis=0), rows_local)
+    position = jnp.sum(jnp.where(chosen, count[None], 0.0), axis=1)
+    slot = (ids * capacity + position).T.astype(jnp.int32)
+    columns = jnp.arange(experts * capacity, dtype=jnp.int32)[None, :]
+    spread = jnp.zeros((rows_local, experts * capacity), jnp.float32)
+    for k in range(TOP_K):
+        spread = spread + jnp.where(
+            slot[:, k : k + 1] == columns, routed_expert_weight[:, k : k + 1], 0.0
+        )
+    high = lax.reduce_precision(spread, 8, 7)
+    low = (spread - high).astype(jnp.bfloat16)
+    routed_sum = jnp.dot(
+        high.astype(jnp.bfloat16), returned, preferred_element_type=jnp.float32
+    ) + jnp.dot(low, returned, preferred_element_type=jnp.float32)
     shared_result = jnp.dot(whole_shared, shared_down_weight, preferred_element_type=jnp.float32)
     routed_out = (routed_sum + shared_result).astype(jnp.bfloat16)
     return (mixer_output, routed_out)

time: 294 us -> 247 us (0.84)
  blocking collectives: 81.7 us -> 0 us
  starting transfers between devices: 7.51 us -> 37.5 us
  waiting for transfers between devices: 69.8 us -> 97.1 us
  local copies, waits for them, and re-layouts: 55.5 us -> 29.6 us
  matrix products: 32.9 us -> 37.5 us
    all_to_all x1 -> x0, blocking collectives: 43.9 us -> none  [on_device(): lax.all_to_all(my_columns, 'ep', split_axis=0, concat_axis=1, tiled=True)]
    ppermute x1 -> x8, starting transfers between devices: 2.18 us -> 32.6 us  [passed_along(): return lax.ppermute(x, axis, pairs)]
    all_gather x3, waiting for transfers between devices: 28.2 us -> 52.6 us  [the longest x1 26.7 us: on_device(): whole_mix = lax.all_gather(mixer_normed, 'tp', axis=1, tiled=True)]
    all_gather x1 -> x0, blocking collectives: 20.6 us -> none  [on_device(): lax.all_gather(shared_hidden, 'tp', axis=1, tiled=True)]
    unnamed x1 -> x0, blocking collectives: 17.1 us -> none
    gather x3 -> x0, local copies, waits for them, and re-layouts: 13.7 us -> none  [the longest x1 7.02 us: on_device(): jnp.take(padded, slot_owner, axis=0).reshape(experts, capacity, model_width)]
    dot_general x0 -> x6, matrix products: none -> 8.2 us  [the longest x2 2.78 us: on_device(): jnp.einsum('bsr,brd->bsd', pick[:, j], their_rows, preferred_element_type...]
    ppermute x1 -> x8, waiting for transfers between devices: 0.01 us -> 6.47 us  [passed_along(): return lax.ppermute(x, axis, pairs)]
  transfers between devices with their start and end apart: 6 -> 13, of which waited for: 4 -> 9; matrix products, arithmetic and copies ran while one was open for 26% -> 28% of each run, Pallas kernels for 0% -> 0%
where the time goes in v1:
time: 247 us; the launch traced here: 246 us
  waiting for transfers between devices  97.1 us (39%)
  starting transfers between devices  37.5 us (15%)
  matrix products  37.5 us (15%)
  local copies, waits for them, and re-layouts  29.6 us (12%)
  other arithmetic  29.6 us (12%)
  between operations  14.5 us (6%)
    ppermute x8, starting transfers between devices, passed_along(): return lax.ppermute(x, axis, pairs)  32.6 us
    all_gather x1, waiting for transfers between devices, on_device(): column_piece = lax.all_gather(arrived, 'tp', axis=2, tiled=True)  31.8 us
    all_gather x1, waiting for transfers between devices, on_device(): whole_mix = lax.all_gather(mixer_normed, 'tp', axis=1, tiled=True)  26.7 us
    all_gather x1, waiting for transfers between devices, on_device(): whole_rows = lax.all_gather(hidden_rows, 'tp', axis=1, tiled=True)  25.2 us
    ppermute x8, waiting for transfers between devices, passed_along(): return lax.ppermute(x, axis, pairs)  6.47 us
    all_to_all x1, waiting for transfers between devices, on_device(): lax.all_to_all(going, 'ep', split_axis=0, concat_axis=0, tiled=True)  6.17 us
    unnamed x73, local copies, waits for them, and re-layouts  5.5 us
    dot_general x1, matrix products, on_device(): jnp.einsum('esd,edf->esf', column_piece, routed_gate_weight, preferred_el...  5.34 us
  transfers between devices with their start and end apart: 13, of which 9 were waited for; matrix products, arithmetic and copies ran while one was open for 28% of the time, Pallas kernels for 0%

profile of v1, /device:TPU:0, one launch (start us, length us, event | category | flops | bytes accessed | tf_op | source)
XLA Modules:
  0.0 245.8 jit_solution(2947005200692438754)
XLA Ops:
  10.7 3.2 %collective-permute-start = (bf16[3,2048]{0,1:T(8,128)(2,1)}, bf16[3,2048]{0,1:T(8,128)(2,1)}, u32[]{:S(2)}, u32[]{:S(2)}) collective-permute-start(bf16[3,2048]{0,1:T(8,128)(2,1)} %copy.76), channel_id=1, source_target_pairs={{0,4},{4,8},{8,12},{12,16},{16,20},{20,24},{24,28},{1,5},{5,9},{9,... | collective-permute-start | bytes 36872 | tf_op jit(solution)/shard_map/ppermute | solution.py:20
  28.1 3.4 %multiply_convert_fusion.2 = (bf16[256,512]{1,0:T(8,128)(2,1)}, bf16[256,512]{1,0:T(8,128)(2,1)}) fusion(bf16[256,512]{1,0:T(8,128)(2,1)} %param.26, bf16[3,512]{1,0:T(4,128)(2,1)} %copy.80, f32[512]{0:T(512)} %bitcast.137, f32[512]{0:T(512)} %bitcast.138, f32[512]{0:T(512)} %bitcast.136, f32[512]{0:T(512)} %bitcast.135, f32[512]{0:T(512)} %bitcast.141, ...), kind=kLoop, calls=%fused_computation.104 | loop fusion | flops 6553600 | bytes 1071104 | tf_op jit(solution)/shard_map/convert_element_type | solution.py:46
  34.4 2.9 %fusion.72 = f32[256,1024]{0,1:T(8,128)} fusion(f32[1024]{0:T(1024)} %bitcast.130, bf16[256,1024]{0,1:T(8,128)(2,1)S(1)} %copy.77, f32[1024]{0:T(1024)} %bitcast.131, bf16[3,1024]{0,1:T(8,128)(2,1)S(1)} %slice.176, f32[1024]{0:T(1024)} %bitcast.129, f32[1024]{0:T(1024)} %bitcast.128), kind=kLoop, calls=%fused_computation.107 | loop fusion | flops 6815744 | bytes 1595392 | tf_op jit(solution)/shard_map/convert_element_type | solution.py:146
  37.3 2.8 %reshape.129 = f32[2,128,16,64]{1,0,3,2:T(2,128)} reshape(f32[256,1024]{0,1:T(8,128)} %fusion.72) | data formatting | bytes 2097152 | tf_op jit(solution)/shard_map/reshape | solution.py:146
  40.0 3.0 %broadcast_multiply_fusion = (f32[2,128,16,64]{1,0,3,2:T(2,128)S(1)}, f32[2,128,16,64]{1,0,3,2:T(2,128)}) fusion(f32[2,128,16]{1,0,2:T(2,128)S(1)} %copy.87, f32[2,128,16,64]{1,0,3,2:T(2,128)} %reshape.129, f32[2,128,16]{1,0,2:T(2,128)S(1)} %copy-done.14), kind=kLoop, calls=%fused_computation.103 | loop fusion | flops 524288 | bytes 3178496 | tf_op jit(solution)/shard_map/bjhn,bjh,bjhp->bhpn/dot_general | solution.py:162
  43.3 3.1 %fusion.37 = f32[2,16,64,128]{3,2,1,0:T(8,128)} fusion(f32[2,128,16,128]{3,1,2,0:T(8,128)S(1)} %bitcast.118, f32[2,128,16,64]{1,0,3,2:T(2,128)S(1)} %get-tuple-element.78), kind=kOutput, calls=%fused_computation.55 | convolution fusion | flops 402653184 | bytes 4194304 | tf_op jit(solution)/shard_map/bjhn,bjh,bjhp->bhpn/dot_general | solution.py:162
  46.4 4.1 %while.13 = (s32[]{:T(128)}, f32[16,64,128]{2,1,0:T(8,128)S(1)}, f32[2,16,64,128]{3,2,1,0:T(8,128)}, f32[2,16]{1,0:T(2,128)S(1)}, f32[2,16,64,128]{3,2,1,0:T(8,128)}, /*index=5*/s32[]{:T(128)}, s32[]{:T(128)}) while((s32[]{:T(128)}, f32[16,64,128]{2,1,0:T(8,128)S(1)}, f32[2,16,64,128]{3,2,1,0:T(8,128)}, f32[2,16]{1,0:T(2,128)S(1)}, ...), condition=%wide.region_3.4_spmd.clone, body=%wide.region_2.3_spmd.clone.sunk | while | flops 524291 | bytes 2621740 | solution.py:164
  56.9 3.1 %collective-permute-start.1 = (bf16[16,64,128]{2,1,0:T(8,128)(2,1)S(1)}, bf16[16,64,128]{2,1,0:T(8,128)(2,1)S(1)}, u32[]{:S(2)}, u32[]{:S(2)}) collective-permute-start(bf16[16,64,128]{2,1,0:T(8,128)(2,1)S(1)} %convert_element_type.179), channel_id=1, source_target_pairs={{0,4},{4,8},{8,12},{12,16},{16,20},{20,24},{24,28},{1,5},{5,9},{9,... | collective-permute-start | bytes 786440 | tf_op jit(solution)/shard_map/ppermute | solution.py:20
  61.1 4.4 %collective-permute-start.3 = (bf16[16,64,128]{2,1,0:T(8,128)(2,1)S(1)}, bf16[16,64,128]{2,1,0:T(8,128)(2,1)S(1)}, u32[]{:S(2)}, u32[]{:S(2)}) collective-permute-start(bf16[16,64,128]{2,1,0:T(8,128)(2,1)S(1)} %collective-permute-done.1), channel_id=1, source_target_pairs={{0,4},{4,8},{8,12},{12,16},{16,20},{20,24},{24,28},{1,5},{5,9},{9,... | collective-permute-start | bytes 786440 | tf_op jit(solution)/shard_map/ppermute | solution.py:20
  65.6 4.4 %collective-permute-start.2 = (f32[16]{0:T(128)S(1)}, f32[16]{0:T(128)S(1)}, u32[]{:S(2)}, u32[]{:S(2)}) collective-permute-start(f32[16]{0:T(128)S(1)} %copy-done.30), channel_id=1, source_target_pairs={{0,4},{4,8},{8,12},{12,16},{16,20},{20,24},{24,28},{1,5},{5,9},{9,... | collective-permute-start | bytes 200 | tf_op jit(solution)/shard_map/ppermute | solution.py:20
  74.3 6.6 %collective-permute-start.5 = (bf16[16,64,128]{2,1,0:T(8,128)(2,1)S(1)}, bf16[16,64,128]{2,1,0:T(8,128)(2,1)S(1)}, u32[]{:S(2)}, u32[]{:S(2)}) collective-permute-start(bf16[16,64,128]{2,1,0:T(8,128)(2,1)S(1)} %fusion.73), channel_id=1, source_target_pairs={{0,8},{4,12},{8,16},{12,20},{16,24},{20,28},{1,9},{5,13},{9,17},{1... | collective-permute-start | bytes 786440 | tf_op jit(solution)/shard_map/ppermute | solution.py:20
  82.9 3.1 %collective-permute-start.6 = (f32[16]{0:T(128)S(1)}, f32[16]{0:T(128)S(1)}, u32[]{:S(2)}, u32[]{:S(2)}) collective-permute-start(f32[16]{0:T(128)S(1)} %get-tuple-element.77), channel_id=1, source_target_pairs={{0,8},{4,12},{8,16},{12,20},{16,24},{20,28},{1,9},{5,13},{9,17},{1... | collective-permute-start | bytes 200 | tf_op jit(solution)/shard_map/ppermute | solution.py:20
  86.3 5.2 %collective-permute-start.7 = (bf16[16,64,128]{2,1,0:T(8,128)(2,1)S(1)}, bf16[16,64,128]{2,1,0:T(8,128)(2,1)S(1)}, u32[]{:S(2)}, u32[]{:S(2)}) collective-permute-start(bf16[16,64,128]{2,1,0:T(8,128)(2,1)S(1)} %fusion.75), channel_id=1, source_target_pairs={{0,16},{4,20},{8,24},{12,28},{1,17},{5,21},{9,25},{13,29},{2,18},{... | collective-permute-start | bytes 786440 | tf_op jit(solution)/shard_map/ppermute | solution.py:20
  92.0 3.7 %collective-permute-done.7 = bf16[16,64,128]{2,1,0:T(8,128)(2,1)S(1)} collective-permute-done((bf16[16,64,128]{2,1,0:T(8,128)(2,1)S(1)}, bf16[16,64,128]{2,1,0:T(8,128)(2,1)S(1)}, u32[]{:S(2)}, u32[]{:S(2)}) %collective-permute-start.7) | collective-permute-done | bytes 262176 | tf_op jit(solution)/shard_map/ppermute | solution.py:20
  96.1 31.8 %all-gather.6.cloned.1.call-done = bf16[2,768,2048]{2,1,0:T(8,128)(2,1)} async-done(((bf16[2,768,512]{2,1,0:T(8,128)(2,1)}), bf16[2,768,2048]{2,1,0:T(8,128)(2,1)}) %all-gather.6.cloned.1.call-update) | async-done | bytes 6291472 | tf_op jit(solution)/shard_map/all_gather | solution.py:188
  127.9 5.3 %fusion.101 = f32[2,768,256]{2,1,0:T(8,128)S(1)} fusion(bf16[2,768,2048]{2,1,0:T(8,128)(2,1)} %all-gather.6.cloned.1.call-done, bf16[2,2048,256]{2,1,0:T(8,128)(2,1)} %param.42), kind=kOutput, calls=%fused_computation.161 | convolution fusion | flops 1610612736 | bytes 9961472 | tf_op jit(solution)/shard_map/esd,edf->esf/dot_general | solution.py:205
  141.9 4.2 %fusion.27 = f32[2,128,16,64]{1,3,2,0:T(8,128)S(1)} fusion(f32[2,128,16,128]{3,1,2,0:T(8,128)S(1)} %bitcast.119, f32[2,16,64,128]{3,2,1,0:T(8,128)S(1)} %copy-done.12, f32[2,128,16]{1,2,0:T(8,128)S(1)} %copy.92, f32[16,64,128]{2,1,0:T(8,128)S(1)} %multiply_add_fusion, f32[2,16]{1,0:T(2,128)S(1)} %copy-done.26), kind=kOutput, calls=%fused_computation.37 | convolution fusion | flops 403439616 | bytes 4735104 | tf_op jit(solution)/shard_map/bihn,bhpn->bihp/dot_general | solution.py:192
  147.3 4.3 %fusion.24 = f32[2,128,16,64]{1,3,2,0:T(8,128)S(1)} fusion(f32[2,128,16,64]{1,3,2,0:T(8,128)S(1)} %fusion.27, f32[2,16,128,128]{3,2,1,0:T(8,128)S(1)} %bitcast.117, f32[2,128,16,64]{1,0,3,2:T(2,128)S(1)} %copy-done.6, f32[2,16,128]{2,1,0:T(8,128)S(1)} %copy.84, pred[128,128]{1,0:T(8,128)(4,1)S(1)} %iota_compare_fusion.9), kind=kOutput, calls=%fused_computation.35 | convolution fusion | flops 405012480 | bytes 5275648 | tf_op jit(solution)/shard_map/bhij,bjhp->bihp/dot_general | solution.py:157
  153.4 3.1 %reshape.137 = f32[256,4,256]{0,2,1:T(8,128)} reshape(f32[2,128,16,64]{1,0,3,2:T(2,128)} %copy.93) | data formatting | bytes 2097152 | tf_op jit(solution)/shard_map/reshape | solution.py:195
  159.8 25.2 %all-gather.10.cloned.1.call-done = bf16[1792,1024]{1,0:T(8,128)(2,1)} async-done(((bf16[1792,256]{1,0:T(8,128)(2,1)}), bf16[1792,1024]{1,0:T(8,128)(2,1)}) %all-gather.10.cloned.1.call-update) | async-done | bytes 3670032 | tf_op jit(solution)/shard_map/all_gather | solution.py:220
  190.2 4.8 %all-to-all-start = ((bf16[8,192,512]{2,1,0:T(8,128)(2,1)}), bf16[8,192,512]{2,1,0:T(8,128)(2,1)}, u32[]{:S(2)}, u32[]{:S(2)}) async-start(bf16[8,192,512]{2,1,0:T(8,128)(2,1)} %pad_maximum_fusion.1), calls=%async_computation | async-start | bytes 3145728 | tf_op jit(solution)/shard_map/all_to_all | solution.py:234
  195.2 26.7 %all-gather.8.cloned.1.call-done = bf16[256,4096]{0,1:T(8,128)(2,1)} async-done(((bf16[256,1024]{0,1:T(8,128)(2,1)}), bf16[256,4096]{0,1:T(8,128)(2,1)}) %all-gather.8.cloned.1.call-update) | async-done | bytes 2097168 | tf_op jit(solution)/shard_map/all_gather | solution.py:223
  221.9 4.8 %convolution_convert_fusion.1 = bf16[256,512]{1,0:T(8,128)(2,1)} fusion(bf16[256,4096]{0,1:T(8,128)(2,1)} %all-gather.8.cloned.1.call-done, bf16[4096,512]{1,0:T(8,128)(2,1)} %param.37), kind=kOutput, calls=%fused_computation.43 | convolution fusion | flops 1073872896 | bytes 6553600 | tf_op jit(solution)/shard_map/dot_general | solution.py:224
  226.7 6.2 %all-to-all-done = bf16[8,192,512]{2,1,0:T(8,128)(2,1)} async-done(((bf16[8,192,512]{2,1,0:T(8,128)(2,1)}), bf16[8,192,512]{2,1,0:T(8,128)(2,1)}, u32[]{:S(2)}, u32[]{:S(2)}) %all-to-all-start) | async-done | bytes 1572896 | tf_op jit(solution)/shard_map/all_to_all | solution.py:234
  (181 shorter events, 66.1 us)
Async XLA Ops:
  7.2 177.8 %copy-start = (bf16[2,1024,512]{2,1,0:T(8,128)(2,1)S(1)}, bf16[2,1024,512]{2,1,0:T(8,128)(2,1)}, u32[]{:S(2)}) copy-start(bf16[2,1024,512]{2,1,0:T(8,128)(2,1)} %param.44) | copy-start | bytes 6291460
  7.2 9.6 %copy-start.7 = (bf16[256,2048]{1,0:T(8,128)(2,1)S(1)}, bf16[256,2048]{1,0:T(8,128)(2,1)}, u32[]{:S(2)}) copy-start(bf16[256,2048]{1,0:T(8,128)(2,1)} %param.38) | copy-start | bytes 3145732
  7.2 44.0 %all-gather.12.cloned.1.call-start = ((), (), s32[]{:S(2)}) async-start(), calls=%async_computation.4 | async-start | bytes 2433024 | tf_op jit(solution)/shard_map/all_gather | solution.py:135
  10.7 15.6 %collective-permute-start = (bf16[3,2048]{0,1:T(8,128)(2,1)}, bf16[3,2048]{0,1:T(8,128)(2,1)}, u32[]{:S(2)}, u32[]{:S(2)}) collective-permute-start(bf16[3,2048]{0,1:T(8,128)(2,1)} %copy.76), channel_id=1, source_target_pairs={{0,4},{4,8},{8,12},{12,16},{16,20},{20,24},{24,28},{1,5},{5,9},{9,... | collective-permute-start | bytes 36872 | tf_op jit(solution)/shard_map/ppermute | solution.py:20
  16.7 5.2 %copy-start.23 = (f32[4,512]{1,0:T(4,128)S(1)}, f32[4,512]{1,0:T(4,128)}, u32[]{:S(2)}) copy-start(f32[4,512]{1,0:T(4,128)} %param.35) | copy-start | bytes 24580
  16.7 5.8 %copy-start.19 = (f32[4,1024]{1,0:T(4,128)S(1)}, f32[4,1024]{1,0:T(4,128)}, u32[]{:S(2)}) copy-start(f32[4,1024]{1,0:T(4,128)} %param.33) | copy-start | bytes 49156
  19.6 108.3 %all-gather.6.cloned.1.call-start = ((), (), s32[]{:S(2)}) async-start(), calls=%async_computation.1 | async-start | bytes 7864320 | tf_op jit(solution)/shard_map/all_gather | solution.py:188
  46.4 5.8 %copy-start.28 = (f32[2]{0:T(128)S(1)}, f32[2]{0:T(128)}, u32[]{:S(2)}) copy-start(f32[2]{0:T(128)} %add_convert_fusion) | copy-start | bytes 28
  56.8 8.8 %copy-start.30 = (f32[16]{0:T(128)S(1)}, f32[16]{0:T(128)}, u32[]{:S(2)}) copy-start(f32[16]{0:T(128)} %get-tuple-element.84) | copy-start | bytes 196
  56.8 128.2 %all-gather.10.cloned.1.call-start = ((), (), s32[]{:S(2)}) async-start(), calls=%async_computation.3 | async-start | bytes 4587520 | tf_op jit(solution)/shard_map/all_gather | solution.py:220
  56.9 4.3 %collective-permute-start.1 = (bf16[16,64,128]{2,1,0:T(8,128)(2,1)S(1)}, bf16[16,64,128]{2,1,0:T(8,128)(2,1)S(1)}, u32[]{:S(2)}, u32[]{:S(2)}) collective-permute-start(bf16[16,64,128]{2,1,0:T(8,128)(2,1)S(1)} %convert_element_type.179), channel_id=1, source_target_pairs={{0,4},{4,8},{8,12},{12,16},{16,20},{20,24},{24,28},{1,5},{5,9},{9,... | collective-permute-start | bytes 786440 | tf_op jit(solution)/shard_map/ppermute | solution.py:20
  61.1 12.9 %collective-permute-start.3 = (bf16[16,64,128]{2,1,0:T(8,128)(2,1)S(1)}, bf16[16,64,128]{2,1,0:T(8,128)(2,1)S(1)}, u32[]{:S(2)}, u32[]{:S(2)}) collective-permute-start(bf16[16,64,128]{2,1,0:T(8,128)(2,1)S(1)} %collective-permute-done.1), channel_id=1, source_target_pairs={{0,4},{4,8},{8,12},{12,16},{16,20},{20,24},{24,28},{1,5},{5,9},{9,... | collective-permute-start | bytes 786440 | tf_op jit(solution)/shard_map/ppermute | solution.py:20
  65.6 5.2 %collective-permute-start.2 = (f32[16]{0:T(128)S(1)}, f32[16]{0:T(128)S(1)}, u32[]{:S(2)}, u32[]{:S(2)}) collective-permute-start(f32[16]{0:T(128)S(1)} %copy-done.30), channel_id=1, source_target_pairs={{0,4},{4,8},{8,12},{12,16},{16,20},{20,24},{24,28},{1,5},{5,9},{9,... | collective-permute-start | bytes 200 | tf_op jit(solution)/shard_map/ppermute | solution.py:20
  70.8 3.3 %collective-permute-start.4 = (f32[16]{0:T(128)S(1)}, f32[16]{0:T(128)S(1)}, u32[]{:S(2)}, u32[]{:S(2)}) collective-permute-start(f32[16]{0:T(128)S(1)} %collective-permute-done.2), channel_id=1, source_target_pairs={{0,4},{4,8},{8,12},{12,16},{16,20},{20,24},{24,28},{1,5},{5,9},{9,... | collective-permute-start | bytes 200 | tf_op jit(solution)/shard_map/ppermute | solution.py:20
  74.2 17.3 %copy-start.4 = (bf16[256,2048]{1,0:T(8,128)(2,1)S(1)}, bf16[256,2048]{1,0:T(8,128)(2,1)}, u32[]{:S(2)}) copy-start(bf16[256,2048]{1,0:T(8,128)(2,1)} %copy-done.3) | copy-start | bytes 3145732
  74.3 17.3 %copy-start.34 = (bf16[2048,256]{1,0:T(8,128)(2,1)S(1)}, bf16[2048,256]{1,0:T(8,128)(2,1)}, u32[]{:S(2)}) copy-start(bf16[2048,256]{1,0:T(8,128)(2,1)} %param.46) | copy-start | bytes 3145732
  74.3 11.7 %collective-permute-start.5 = (bf16[16,64,128]{2,1,0:T(8,128)(2,1)S(1)}, bf16[16,64,128]{2,1,0:T(8,128)(2,1)S(1)}, u32[]{:S(2)}, u32[]{:S(2)}) collective-permute-start(bf16[16,64,128]{2,1,0:T(8,128)(2,1)S(1)} %fusion.73), channel_id=1, source_target_pairs={{0,8},{4,12},{8,16},{12,20},{16,24},{20,28},{1,9},{5,13},{9,17},{1... | collective-permute-start | bytes 786440 | tf_op jit(solution)/shard_map/ppermute | solution.py:20
  82.9 9.1 %collective-permute-start.6 = (f32[16]{0:T(128)S(1)}, f32[16]{0:T(128)S(1)}, u32[]{:S(2)}, u32[]{:S(2)}) collective-permute-start(f32[16]{0:T(128)S(1)} %get-tuple-element.77), channel_id=1, source_target_pairs={{0,8},{4,12},{8,16},{12,20},{16,24},{20,28},{1,9},{5,13},{9,17},{1... | collective-permute-start | bytes 200 | tf_op jit(solution)/shard_map/ppermute | solution.py:20
  86.3 9.5 %collective-permute-start.7 = (bf16[16,64,128]{2,1,0:T(8,128)(2,1)S(1)}, bf16[16,64,128]{2,1,0:T(8,128)(2,1)S(1)}, u32[]{:S(2)}, u32[]{:S(2)}) collective-permute-start(bf16[16,64,128]{2,1,0:T(8,128)(2,1)S(1)} %fusion.75), channel_id=1, source_target_pairs={{0,16},{4,20},{8,24},{12,28},{1,17},{5,21},{9,25},{13,29},{2,18},{... | collective-permute-start | bytes 786440 | tf_op jit(solution)/shard_map/ppermute | solution.py:20
  127.9 5.4 %copy-start.32 = (bf16[2,768,2048]{2,1,0:T(8,128)(2,1)S(1)}, bf16[2,768,2048]{2,1,0:T(8,128)(2,1)}, u32[]{:S(2)}) copy-start(bf16[2,768,2048]{2,1,0:T(8,128)(2,1)} %all-gather.6.cloned.1.call-done) | copy-start | bytes 18874372
  127.9 5.8 %copy-start.33 = (bf16[2,2048,256]{2,1,0:T(8,128)(2,1)S(1)}, bf16[2,2048,256]{2,1,0:T(8,128)(2,1)}, u32[]{:S(2)}) copy-start(bf16[2,2048,256]{2,1,0:T(8,128)(2,1)} %param.43) | copy-start | bytes 6291460
  136.8 85.1 %all-gather.8.cloned.1.call-start = ((), (), s32[]{:S(2)}) async-start(), calls=%async_computation.2 | async-start | bytes 2621440 | tf_op jit(solution)/shard_map/all_gather | solution.py:223
  190.2 5.0 %copy-start.18 = (s32[256,4]{0,1:T(4,128)S(1)}, s32[256,4]{0,1:T(4,128)}, u32[]{:S(2)}) copy-start(s32[256,4]{0,1:T(4,128)} %param.40) | copy-start | bytes 12292
  190.2 42.7 %all-to-all-start = ((bf16[8,192,512]{2,1,0:T(8,128)(2,1)}), bf16[8,192,512]{2,1,0:T(8,128)(2,1)}, u32[]{:S(2)}, u32[]{:S(2)}) async-start(bf16[8,192,512]{2,1,0:T(8,128)(2,1)} %pad_maximum_fusion.1), calls=%async_computation | async-start | bytes 3145728 | tf_op jit(solution)/shard_map/all_to_all | solution.py:234
  (26 other events, 77.9 us)
Sparse Core Ops, SparseCore 0:
  19.7 31.4 all-gather.11
  56.9 70.9 all-gather.5
  136.9 48.0 all-gather.9
  186.7 35.1 all-gather.7

commit v2 on v1

--- a/solution.py
+++ b/solution.py
@@ -213,14 +213,12 @@
         jax.nn.silu(jnp.dot(normed, shared_gate_weight, preferred_element_type=jnp.float32))
         * jnp.dot(normed, shared_up_weight, preferred_element_type=jnp.float32)
     ).astype(jnp.bfloat16)
-    slots = ep_count * capacity
-    hidden_rows = jnp.concatenate(
-        [hidden.reshape(local_experts * slots, hidden.shape[2]), shared_hidden], axis=0
-    )
-    whole_rows = lax.all_gather(hidden_rows, "tp", axis=1, tiled=True)
-    whole_hidden = whole_rows[: local_experts * slots].reshape(local_experts, slots, -1)
-    whole_shared = whole_rows[local_experts * slots :]
-    whole_mix = lax.all_gather(mixer_normed, "tp", axis=1, tiled=True)
+    whole_hidden = lax.all_gather(hidden, "tp", axis=2, tiled=True)
+    both = lax.all_gather(
+        jnp.concatenate([mixer_normed, shared_hidden], axis=1), "tp", axis=1, tiled=True
+    ).reshape(length, lax.axis_size("tp"), -1)
+    whole_mix = both[:, :, :width_x].reshape(length, -1)
+    whole_shared = both[:, :, width_x:].reshape(length, -1)
     mixer_output = jnp.dot(
         whole_mix, mixer_output_weight, preferred_element_type=jnp.float32
     ).astype(jnp.bfloat16)

time: 247 us -> 241 us (0.976)
  waiting for transfers between devices: 97.1 us -> 87.8 us
  local copies, waits for them, and re-layouts: 29.6 us -> 34.6 us
    all_gather x2, waiting for transfers between devices: 51.8 us -> 45.6 us  [the longest x1 30.9 us: on_device(): lax.all_gather(jnp.concatenate([mixer_normed, shared_hidden], axis=1), 't...]
    all_to_all x1, waiting for transfers between devices: 6.17 us -> 0.87 us  [on_device(): lax.all_to_all(going, 'ep', split_axis=0, concat_axis=0, tiled=True)]
    ppermute x8, waiting for transfers between devices: 6.47 us -> 9.39 us  [passed_along(): return lax.ppermute(x, axis, pairs)]
    dot_general x1, matrix products: 4.79 us -> 1.97 us  [on_device(): jnp.dot(whole_mix, mixer_output_weight, preferred_element_type=jnp.float32)]
    unnamed x73 -> x77, local copies, waits for them, and re-layouts: 5.5 us -> 6.78 us
  transfers between devices with their start and end apart: 13 -> 13, of which waited for: 9 -> 10; matrix products, arithmetic and copies ran while one was open for 28% -> 30% of each run, Pallas kernels for 0% -> 0%
where the time goes in v2:
time: 241 us; the launch traced here: 240 us
  waiting for transfers between devices  87.8 us (36%)
  matrix products  37.4 us (16%)
  starting transfers between devices  36.9 us (15%)
  local copies, waits for them, and re-layouts  34.6 us (14%)
  other arithmetic  28.6 us (12%)
  between operations  14.4 us (6%)
    ppermute x8, starting transfers between devices, passed_along(): return lax.ppermute(x, axis, pairs)  32 us
    all_gather x1, waiting for transfers between devices, on_device(): column_piece = lax.all_gather(arrived, 'tp', axis=2, tiled=True)  31.1 us
    all_gather x1, waiting for transfers between devices, on_device(): lax.all_gather(jnp.concatenate([mixer_normed, shared_hidden], axis=1), 't...  30.9 us
    all_gather x1, waiting for transfers between devices, on_device(): whole_hidden = lax.all_gather(hidden, 'tp', axis=2, tiled=True)  14.7 us
    ppermute x8, waiting for transfers between devices, passed_along(): return lax.ppermute(x, axis, pairs)  9.39 us
    unnamed x77, local copies, waits for them, and re-layouts  6.78 us
    dot_general x1, matrix products, on_device(): jnp.einsum('esd,edf->esf', column_piece, routed_gate_weight, preferred_el...  5.34 us
  transfers between devices with their start and end apart: 13, of which 10 were waited for; matrix products, arithmetic and copies ran while one was open for 30% of the time, Pallas kernels for 0%

profile of v2, /device:TPU:0, one launch (start us, length us, event | category | flops | bytes accessed | tf_op | source)
XLA Modules:
  0.0 239.8 jit_solution(12581473368572431942)
XLA Ops:
  10.7 3.2 %collective-permute-start = (bf16[3,2048]{0,1:T(8,128)(2,1)}, bf16[3,2048]{0,1:T(8,128)(2,1)}, u32[]{:S(2)}, u32[]{:S(2)}) collective-permute-start(bf16[3,2048]{0,1:T(8,128)(2,1)} %copy.77), channel_id=1, source_target_pairs={{0,4},{4,8},{8,12},{12,16},{16,20},{20,24},{24,28},{1,5},{5,9},{9,... | collective-permute-start | bytes 36872 | tf_op jit(solution)/shard_map/ppermute | solution.py:20
  26.7 3.4 %multiply_convert_fusion.2 = (bf16[256,512]{1,0:T(8,128)(2,1)}, bf16[256,512]{1,0:T(8,128)(2,1)}) fusion(bf16[256,512]{1,0:T(8,128)(2,1)} %param.26, bf16[3,512]{1,0:T(4,128)(2,1)} %copy.81, f32[512]{0:T(512)} %bitcast.141, f32[512]{0:T(512)} %bitcast.142, f32[512]{0:T(512)} %bitcast.140, f32[512]{0:T(512)} %bitcast.139, f32[512]{0:T(512)} %bitcast.145, ...), kind=kLoop, calls=%fused_computation.103 | loop fusion | flops 6553600 | bytes 1071104 | tf_op jit(solution)/shard_map/convert_element_type | solution.py:46
  32.9 2.9 %fusion.71 = f32[256,1024]{0,1:T(8,128)} fusion(f32[1024]{0:T(1024)} %bitcast.134, bf16[256,1024]{0,1:T(8,128)(2,1)S(1)} %copy.78, f32[1024]{0:T(1024)} %bitcast.135, bf16[3,1024]{0,1:T(8,128)(2,1)S(1)} %slice.176, f32[1024]{0:T(1024)} %bitcast.133, f32[1024]{0:T(1024)} %bitcast.132), kind=kLoop, calls=%fused_computation.106 | loop fusion | flops 6815744 | bytes 1595392 | tf_op jit(solution)/shard_map/convert_element_type | solution.py:146
  35.8 2.7 %reshape.132 = f32[2,128,16,64]{1,0,3,2:T(2,128)} reshape(f32[256,1024]{0,1:T(8,128)} %fusion.71) | data formatting | bytes 2097152 | tf_op jit(solution)/shard_map/reshape | solution.py:146
  38.6 3.0 %broadcast_multiply_fusion = (f32[2,128,16,64]{1,0,3,2:T(2,128)S(1)}, f32[2,128,16,64]{1,0,3,2:T(2,128)}) fusion(f32[2,128,16]{1,0,2:T(2,128)S(1)} %copy.88, f32[2,128,16,64]{1,0,3,2:T(2,128)} %reshape.132, f32[2,128,16]{1,0,2:T(2,128)} %mul.326), kind=kLoop, calls=%fused_computation.102 | loop fusion | flops 524288 | bytes 3178496 | tf_op jit(solution)/shard_map/bjhn,bjh,bjhp->bhpn/dot_general | solution.py:162
  41.8 3.1 %fusion.37 = f32[2,16,64,128]{3,2,1,0:T(8,128)} fusion(f32[2,128,16,128]{3,1,2,0:T(8,128)S(1)} %bitcast.120, f32[2,128,16,64]{1,0,3,2:T(2,128)S(1)} %get-tuple-element.78), kind=kOutput, calls=%fused_computation.55 | convolution fusion | flops 402653184 | bytes 4194304 | tf_op jit(solution)/shard_map/bjhn,bjh,bjhp->bhpn/dot_general | solution.py:162
  44.9 4.0 %while.13 = (s32[]{:T(128)}, f32[16,64,128]{2,1,0:T(8,128)S(1)}, f32[2,16,64,128]{3,2,1,0:T(8,128)}, f32[2,16]{1,0:T(2,128)S(1)}, f32[2,16,64,128]{3,2,1,0:T(8,128)}, /*index=5*/s32[]{:T(128)}, s32[]{:T(128)}) while((s32[]{:T(128)}, f32[16,64,128]{2,1,0:T(8,128)S(1)}, f32[2,16,64,128]{3,2,1,0:T(8,128)}, f32[2,16]{1,0:T(2,128)S(1)}, ...), condition=%wide.region_3.4_spmd.clone, body=%wide.region_2.3_spmd.clone.sunk | while | flops 524291 | bytes 2621740 | solution.py:164
  55.5 3.0 %collective-permute-start.1 = (bf16[16,64,128]{2,1,0:T(8,128)(2,1)S(1)}, bf16[16,64,128]{2,1,0:T(8,128)(2,1)S(1)}, u32[]{:S(2)}, u32[]{:S(2)}) collective-permute-start(bf16[16,64,128]{2,1,0:T(8,128)(2,1)S(1)} %convert_element_type.179), channel_id=1, source_target_pairs={{0,4},{4,8},{8,12},{12,16},{16,20},{20,24},{24,28},{1,5},{5,9},{9,... | collective-permute-start | bytes 786440 | tf_op jit(solution)/shard_map/ppermute | solution.py:20
  59.7 4.5 %collective-permute-start.3 = (bf16[16,64,128]{2,1,0:T(8,128)(2,1)S(1)}, bf16[16,64,128]{2,1,0:T(8,128)(2,1)S(1)}, u32[]{:S(2)}, u32[]{:S(2)}) collective-permute-start(bf16[16,64,128]{2,1,0:T(8,128)(2,1)S(1)} %collective-permute-done.1), channel_id=1, source_target_pairs={{0,4},{4,8},{8,12},{12,16},{16,20},{20,24},{24,28},{1,5},{5,9},{9,... | collective-permute-start | bytes 786440 | tf_op jit(solution)/shard_map/ppermute | solution.py:20
  64.2 4.4 %collective-permute-start.2 = (f32[16]{0:T(128)S(1)}, f32[16]{0:T(128)S(1)}, u32[]{:S(2)}, u32[]{:S(2)}) collective-permute-start(f32[16]{0:T(128)S(1)} %copy-done.31), channel_id=1, source_target_pairs={{0,4},{4,8},{8,12},{12,16},{16,20},{20,24},{24,28},{1,5},{5,9},{9,... | collective-permute-start | bytes 200 | tf_op jit(solution)/shard_map/ppermute | solution.py:20
  72.9 6.5 %collective-permute-start.5 = (bf16[16,64,128]{2,1,0:T(8,128)(2,1)S(1)}, bf16[16,64,128]{2,1,0:T(8,128)(2,1)S(1)}, u32[]{:S(2)}, u32[]{:S(2)}) collective-permute-start(bf16[16,64,128]{2,1,0:T(8,128)(2,1)S(1)} %fusion.72), channel_id=1, source_target_pairs={{0,8},{4,12},{8,16},{12,20},{16,24},{20,28},{1,9},{5,13},{9,17},{1... | collective-permute-start | bytes 786440 | tf_op jit(solution)/shard_map/ppermute | solution.py:20
  79.4 4.6 %collective-permute-done.5 = bf16[16,64,128]{2,1,0:T(8,128)(2,1)S(1)} collective-permute-done((bf16[16,64,128]{2,1,0:T(8,128)(2,1)S(1)}, bf16[16,64,128]{2,1,0:T(8,128)(2,1)S(1)}, u32[]{:S(2)}, u32[]{:S(2)}) %collective-permute-start.5) | collective-permute-done | bytes 262176 | tf_op jit(solution)/shard_map/ppermute | solution.py:20
  84.3 5.4 %collective-permute-start.7 = (bf16[16,64,128]{2,1,0:T(8,128)(2,1)S(1)}, bf16[16,64,128]{2,1,0:T(8,128)(2,1)S(1)}, u32[]{:S(2)}, u32[]{:S(2)}) collective-permute-start(bf16[16,64,128]{2,1,0:T(8,128)(2,1)S(1)} %fusion.74), channel_id=1, source_target_pairs={{0,16},{4,20},{8,24},{12,28},{1,17},{5,21},{9,25},{13,29},{2,18},{... | collective-permute-start | bytes 786440 | tf_op jit(solution)/shard_map/ppermute | solution.py:20
  95.3 31.1 %all-gather.6.cloned.1.call-done = bf16[2,768,2048]{2,1,0:T(8,128)(2,1)} async-done(((bf16[2,768,512]{2,1,0:T(8,128)(2,1)}), bf16[2,768,2048]{2,1,0:T(8,128)(2,1)}) %all-gather.6.cloned.1.call-update) | async-done | bytes 6291472 | tf_op jit(solution)/shard_map/all_gather | solution.py:188
  126.4 5.3 %fusion.101 = f32[2,768,256]{2,1,0:T(8,128)S(1)} fusion(bf16[2,768,2048]{2,1,0:T(8,128)(2,1)} %all-gather.6.cloned.1.call-done, bf16[2,2048,256]{2,1,0:T(8,128)(2,1)} %param.42), kind=kOutput, calls=%fused_computation.161 | convolution fusion | flops 1610612736 | bytes 9961472 | tf_op jit(solution)/shard_map/esd,edf->esf/dot_general | solution.py:205
  132.2 2.9 %multiply_convert_fusion = bf16[2,768,256]{2,1,0:T(8,128)(2,1)} fusion(f32[2,768,256]{2,1,0:T(8,128)S(1)} %fusion.101, bf16[2,768,2048]{2,1,0:T(8,128)(2,1)S(1)} %copy-done.33, bf16[2,2048,256]{2,1,0:T(8,128)(2,1)S(1)} %copy-done.35), kind=kOutput, calls=%fused_computation.25 | convolution fusion | flops 1612972032 | bytes 10747904 | tf_op jit(solution)/shard_map/esd,edf->esf/dot_general | solution.py:208
  146.3 4.2 %fusion.27 = f32[2,128,16,64]{1,3,2,0:T(8,128)S(1)} fusion(f32[2,128,16,128]{3,1,2,0:T(8,128)S(1)} %bitcast.121, f32[2,16,64,128]{3,2,1,0:T(8,128)S(1)} %copy-done.11, f32[2,128,16]{1,2,0:T(8,128)S(1)} %copy-done.13, f32[16,64,128]{2,1,0:T(8,128)S(1)} %copy-done.9, f32[2,16]{1,0:T(2,128)S(1)} %copy-done.27), kind=kOutput, calls=%fused_computation.37 | convolution fusion | flops 403439616 | bytes 4735104 | tf_op jit(solution)/shard_map/bihn,bhpn->bihp/dot_general | solution.py:192
  151.7 4.2 %fusion.24 = f32[2,128,16,64]{1,3,2,0:T(8,128)S(1)} fusion(f32[2,128,16,64]{1,3,2,0:T(8,128)S(1)} %fusion.27, f32[2,16,128,128]{3,2,1,0:T(8,128)S(1)} %bitcast.119, f32[2,128,16,64]{1,0,3,2:T(2,128)S(1)} %copy-done.6, f32[2,16,128]{2,1,0:T(8,128)S(1)} %copy.85, pred[128,128]{1,0:T(8,128)(4,1)S(1)} %copy-done.12), kind=kOutput, calls=%fused_computation.35 | convolution fusion | flops 405012480 | bytes 5275648 | tf_op jit(solution)/shard_map/bhij,bjhp->bihp/dot_general | solution.py:157
  157.7 3.2 %reshape.140 = f32[256,4,256]{0,2,1:T(8,128)} reshape(f32[2,128,16,64]{1,0,3,2:T(2,128)} %copy.94) | data formatting | bytes 2097152 | tf_op jit(solution)/shard_map/reshape | solution.py:195
  164.4 14.7 %all-gather.10.cloned.1.call-done = bf16[2,768,1024]{2,1,0:T(8,128)(2,1)} async-done(((bf16[2,768,256]{2,1,0:T(8,128)(2,1)}), bf16[2,768,1024]{2,1,0:T(8,128)(2,1)}) %all-gather.10.cloned.1.call-update) | async-done | bytes 3145744 | tf_op jit(solution)/shard_map/all_gather | solution.py:216
  179.0 3.7 %convolution_convert_fusion = bf16[2,768,512]{2,1,0:T(8,128)(2,1)S(1)} fusion(bf16[2,768,1024]{2,1,0:T(8,128)(2,1)} %all-gather.10.cloned.1.call-done, bf16[2,1024,512]{2,1,0:T(8,128)(2,1)S(1)} %copy-done), kind=kOutput, calls=%fused_computation.21 | convolution fusion | flops 1611399168 | bytes 6815744 | tf_op jit(solution)/shard_map/esf,efd->esd/dot_general | solution.py:225
  184.4 4.7 %all-to-all-start = ((bf16[8,192,512]{2,1,0:T(8,128)(2,1)}), bf16[8,192,512]{2,1,0:T(8,128)(2,1)}, u32[]{:S(2)}, u32[]{:S(2)}) async-start(bf16[8,192,512]{2,1,0:T(8,128)(2,1)} %pad_maximum_fusion.1), calls=%async_computation | async-start | bytes 3145728 | tf_op jit(solution)/shard_map/all_to_all | solution.py:232
  189.4 30.9 %all-gather.8.cloned.1.call-done = bf16[256,5120]{0,1:T(8,128)(2,1)} async-done(((bf16[256,1280]{0,1:T(8,128)(2,1)}), bf16[256,5120]{0,1:T(8,128)(2,1)}) %all-gather.8.cloned.1.call-update) | async-done | bytes 2621456 | tf_op jit(solution)/shard_map/all_gather | solution.py:217
  229.5 2.6 %convolution_add_fusion.1 = f32[256,512]{1,0:T(8,128)S(1)} fusion(f32[256,512]{1,0:T(8,128)S(1)} %fusion.47, bf16[1536,512]{1,0:T(8,128)(2,1)} %bitcast.43, f32[256]{0:T(256)S(1)} %bitcast.152, s32[256]{0:T(256)S(1)} %bitcast.158, f32[256]{0:T(256)S(1)} %bitcast.154, s32[256]{0:T(256)S(1)} %bitcast.160, f32[256]{0:T(256)S(1)} %bitcast.150, ...), kind=kOutput, calls=%fused_computation.41 | convolution fusion | flops 408289280 | bytes 2629632 | tf_op jit(solution)/shard_map/dot_general | solution.py:249
  (185 shorter events, 71.0 us)
Async XLA Ops:
  7.2 171.9 %copy-start = (bf16[2,1024,512]{2,1,0:T(8,128)(2,1)S(1)}, bf16[2,1024,512]{2,1,0:T(8,128)(2,1)}, u32[]{:S(2)}) copy-start(bf16[2,1024,512]{2,1,0:T(8,128)(2,1)} %param.44) | copy-start | bytes 6291460
  7.2 8.8 %copy-start.7 = (bf16[256,2048]{1,0:T(8,128)(2,1)S(1)}, bf16[256,2048]{1,0:T(8,128)(2,1)}, u32[]{:S(2)}) copy-start(bf16[256,2048]{1,0:T(8,128)(2,1)} %param.38) | copy-start | bytes 3145732
  7.2 8.2 %copy-start.17 = (s32[256,4]{0,1:T(4,128)S(1)}, s32[256,4]{0,1:T(4,128)}, u32[]{:S(2)}) copy-start(s32[256,4]{0,1:T(4,128)} %param.40) | copy-start | bytes 12292
  7.2 8.8 %copy-start.22 = (f32[2048]{0:T(1024)S(1)}, f32[2048]{0:T(1024)}, u32[]{:S(2)}) copy-start(f32[2048]{0:T(1024)} %param.39) | copy-start | bytes 24580
  7.2 42.7 %all-gather.12.cloned.1.call-start = ((), (), s32[]{:S(2)}) async-start(), calls=%async_computation.4 | async-start | bytes 2433024 | tf_op jit(solution)/shard_map/all_gather | solution.py:135
  10.7 14.2 %collective-permute-start = (bf16[3,2048]{0,1:T(8,128)(2,1)}, bf16[3,2048]{0,1:T(8,128)(2,1)}, u32[]{:S(2)}, u32[]{:S(2)}) collective-permute-start(bf16[3,2048]{0,1:T(8,128)(2,1)} %copy.77), channel_id=1, source_target_pairs={{0,4},{4,8},{8,12},{12,16},{16,20},{20,24},{24,28},{1,5},{5,9},{9,... | collective-permute-start | bytes 36872 | tf_op jit(solution)/shard_map/ppermute | solution.py:20
  16.1 5.0 %copy-start.19 = (f32[4,1024]{1,0:T(4,128)S(1)}, f32[4,1024]{1,0:T(4,128)}, u32[]{:S(2)}) copy-start(f32[4,1024]{1,0:T(4,128)} %param.33) | copy-start | bytes 49156
  18.2 108.2 %all-gather.6.cloned.1.call-start = ((), (), s32[]{:S(2)}) async-start(), calls=%async_computation.1 | async-start | bytes 7864320 | tf_op jit(solution)/shard_map/all_gather | solution.py:188
  44.9 5.9 %copy-start.29 = (f32[2]{0:T(128)S(1)}, f32[2]{0:T(128)}, u32[]{:S(2)}) copy-start(f32[2]{0:T(128)} %add_convert_fusion) | copy-start | bytes 28
  55.4 8.8 %copy-start.31 = (f32[16]{0:T(128)S(1)}, f32[16]{0:T(128)}, u32[]{:S(2)}) copy-start(f32[16]{0:T(128)} %get-tuple-element.84) | copy-start | bytes 196
  55.4 123.6 %all-gather.10.cloned.1.call-start = ((), (), s32[]{:S(2)}) async-start(), calls=%async_computation.3 | async-start | bytes 3932160 | tf_op jit(solution)/shard_map/all_gather | solution.py:216
  55.5 4.1 %collective-permute-start.1 = (bf16[16,64,128]{2,1,0:T(8,128)(2,1)S(1)}, bf16[16,64,128]{2,1,0:T(8,128)(2,1)S(1)}, u32[]{:S(2)}, u32[]{:S(2)}) collective-permute-start(bf16[16,64,128]{2,1,0:T(8,128)(2,1)S(1)} %convert_element_type.179), channel_id=1, source_target_pairs={{0,4},{4,8},{8,12},{12,16},{16,20},{20,24},{24,28},{1,5},{5,9},{9,... | collective-permute-start | bytes 786440 | tf_op jit(solution)/shard_map/ppermute | solution.py:20
  59.7 13.1 %collective-permute-start.3 = (bf16[16,64,128]{2,1,0:T(8,128)(2,1)S(1)}, bf16[16,64,128]{2,1,0:T(8,128)(2,1)S(1)}, u32[]{:S(2)}, u32[]{:S(2)}) collective-permute-start(bf16[16,64,128]{2,1,0:T(8,128)(2,1)S(1)} %collective-permute-done.1), channel_id=1, source_target_pairs={{0,4},{4,8},{8,12},{12,16},{16,20},{20,24},{24,28},{1,5},{5,9},{9,... | collective-permute-start | bytes 786440 | tf_op jit(solution)/shard_map/ppermute | solution.py:20
  64.2 5.2 %collective-permute-start.2 = (f32[16]{0:T(128)S(1)}, f32[16]{0:T(128)S(1)}, u32[]{:S(2)}, u32[]{:S(2)}) collective-permute-start(f32[16]{0:T(128)S(1)} %copy-done.31), channel_id=1, source_target_pairs={{0,4},{4,8},{8,12},{12,16},{16,20},{20,24},{24,28},{1,5},{5,9},{9,... | collective-permute-start | bytes 200 | tf_op jit(solution)/shard_map/ppermute | solution.py:20
  69.4 3.3 %collective-permute-start.4 = (f32[16]{0:T(128)S(1)}, f32[16]{0:T(128)S(1)}, u32[]{:S(2)}, u32[]{:S(2)}) collective-permute-start(f32[16]{0:T(128)S(1)} %collective-permute-done.2), channel_id=1, source_target_pairs={{0,4},{4,8},{8,12},{12,16},{16,20},{20,24},{24,28},{1,5},{5,9},{9,... | collective-permute-start | bytes 200 | tf_op jit(solution)/shard_map/ppermute | solution.py:20
  72.9 11.1 %collective-permute-start.5 = (bf16[16,64,128]{2,1,0:T(8,128)(2,1)S(1)}, bf16[16,64,128]{2,1,0:T(8,128)(2,1)S(1)}, u32[]{:S(2)}, u32[]{:S(2)}) collective-permute-start(bf16[16,64,128]{2,1,0:T(8,128)(2,1)S(1)} %fusion.72), channel_id=1, source_target_pairs={{0,8},{4,12},{8,16},{12,20},{16,24},{20,28},{1,9},{5,13},{9,17},{1... | collective-permute-start | bytes 786440 | tf_op jit(solution)/shard_map/ppermute | solution.py:20
  84.3 9.9 %collective-permute-start.7 = (bf16[16,64,128]{2,1,0:T(8,128)(2,1)S(1)}, bf16[16,64,128]{2,1,0:T(8,128)(2,1)S(1)}, u32[]{:S(2)}, u32[]{:S(2)}) collective-permute-start(bf16[16,64,128]{2,1,0:T(8,128)(2,1)S(1)} %fusion.74), channel_id=1, source_target_pairs={{0,16},{4,20},{8,24},{12,28},{1,17},{5,21},{9,25},{13,29},{2,18},{... | collective-permute-start | bytes 786440 | tf_op jit(solution)/shard_map/ppermute | solution.py:20
  89.7 4.5 %collective-permute-start.6 = (f32[16]{0:T(128)S(1)}, f32[16]{0:T(128)S(1)}, u32[]{:S(2)}, u32[]{:S(2)}) collective-permute-start(f32[16]{0:T(128)S(1)} %get-tuple-element.77), channel_id=1, source_target_pairs={{0,8},{4,12},{8,16},{12,20},{16,24},{20,28},{1,9},{5,13},{9,17},{1... | collective-permute-start | bytes 200 | tf_op jit(solution)/shard_map/ppermute | solution.py:20
  126.4 5.4 %copy-start.33 = (bf16[2,768,2048]{2,1,0:T(8,128)(2,1)S(1)}, bf16[2,768,2048]{2,1,0:T(8,128)(2,1)}, u32[]{:S(2)}) copy-start(bf16[2,768,2048]{2,1,0:T(8,128)(2,1)} %all-gather.6.cloned.1.call-done) | copy-start | bytes 18874372
  126.4 5.8 %copy-start.35 = (bf16[2,2048,256]{2,1,0:T(8,128)(2,1)S(1)}, bf16[2,2048,256]{2,1,0:T(8,128)(2,1)}, u32[]{:S(2)}) copy-start(bf16[2,2048,256]{2,1,0:T(8,128)(2,1)} %param.43) | copy-start | bytes 6291460
  135.1 5.9 %copy-start.4 = (bf16[256,2048]{1,0:T(8,128)(2,1)S(1)}, bf16[256,2048]{1,0:T(8,128)(2,1)}, u32[]{:S(2)}) copy-start(bf16[256,2048]{1,0:T(8,128)(2,1)} %copy-done.3) | copy-start | bytes 3145732
  135.2 85.1 %all-gather.8.cloned.1.call-start = ((), (), s32[]{:S(2)}) async-start(), calls=%async_computation.2 | async-start | bytes 3276800 | tf_op jit(solution)/shard_map/all_gather | solution.py:217
  184.4 5.0 %copy-start.18 = (s32[256,4]{0,1:T(4,128)S(1)}, s32[256,4]{0,1:T(4,128)}, u32[]{:S(2)}) copy-start(s32[256,4]{0,1:T(4,128)} %param.40) | copy-start | bytes 12292
  184.4 42.6 %all-to-all-start = ((bf16[8,192,512]{2,1,0:T(8,128)(2,1)}), bf16[8,192,512]{2,1,0:T(8,128)(2,1)}, u32[]{:S(2)}, u32[]{:S(2)}) async-start(bf16[8,192,512]{2,1,0:T(8,128)(2,1)} %pad_maximum_fusion.1), calls=%async_computation | async-start | bytes 3145728 | tf_op jit(solution)/shard_map/all_to_all | solution.py:232
  (27 other events, 67.0 us)
Sparse Core Ops, SparseCore 0:
  18.4 31.4 all-gather.11
  55.5 70.8 all-gather.5
  135.3 43.6 all-gather.9
  180.7 39.4 all-gather.7
